TPU v7x, 32 devices: a whole 2x2x4 slice. The times are simulated.
32 devices in a mesh: ep: 8 (over z, x), tp: 4 (over y, core).
Axes of the slice: x: 2, y: 2, z: 4, core: 2. Of those that a mesh axis runs over, the one named last changes fastest.
Arguments:
- tokens: bfloat16 [128, 2048], P('ep'), may hold values from -6 to 6
- lengths: int32 [128], P('ep'), may hold values from 1 to 1024, as said below
- key_cache: bfloat16 [128, 1024, 8, 128], P('ep', None, 'tp'), may hold values from -200 to 200
- value_cache: bfloat16 [128, 1024, 8, 128], P('ep', None, 'tp'), may hold values from -6 to 6
- attn_gain: float32 [2048], replicated, may hold values from 0.1 to 1.9
- w_query: bfloat16 [2048, 8, 128], P(None, 'tp'), may hold values from -0.1875 to 0.1875
- w_key: bfloat16 [2048, 8, 128], P(None, 'tp'), may hold values from -0.15625 to 0.15625
- w_value: bfloat16 [2048, 8, 128], P(None, 'tp'), may hold values from -0.125 to 0.125
- mix_lambda: float32 [8], P('tp'), may hold values from 0.3 to 0.8
- head_gain: float32 [128], replicated, may hold values from 0.1 to 1.9
- w_out: bfloat16 [8, 128, 2048], P('tp'), may hold values from -2.5 to 2.5
- ffn_gain: float32 [2048], replicated, may hold values from 0.1 to 1.9
- w_gate: bfloat16 [8, 2048, 2048], P('ep', None, 'tp'), may hold values from -1 to 1
- w_up: bfloat16 [8, 2048, 2048], P('ep', None, 'tp'), may hold values from -1 to 1
- w_down: bfloat16 [8, 2048, 2048], P('ep', 'tp'), may hold values from -0.046875 to 0.046875
- routes: int32 [128, 4], P('ep'), may hold values from 0 to 7, all different within a row; in each aligned block of 16 rows (0 to 15, 16 to 31, ...) at most 16 rows name the same one
- route_weights: float32 [128, 4], P('ep'), may hold values from 0.1 to 1
Outputs:
- mixed: bfloat16 [128, 2048], P('ep', 'tp')
Inputs may be any that keep to these rules, and one draw needn't show every extreme that they name: `routes`: in each aligned block of 16 rows no expert is named by more than 16 entries, and one is named by exactly 16 in some block; each row names 4 different experts. `lengths`: some sequence has all 1024 positions valid.
All inputs are finite; a program needn't handle non-finite values.
Results may differ from a plain program's by a relative error of at most 0.02.
The roundings to bfloat16 on the way count: a program that leaves them out, or rounds other values in their place, can miss the bound.
Values may be sent and summed in bfloat16 or wider, within the bound.
No kernel may reach another device: no remote copies, remote signals or barrier semaphores. Data moves between devices by JAX's collectives and lax.ppermute only.
A program may use at most 128 MiB of HBM per device.

v0:
```python
import jax
import jax.numpy as jnp
from jax import lax
from jax.sharding import PartitionSpec as P

epsilon = 1e-06
clamp_limit = 7.0
sigmoid_slope = 1.702
branch_scale = 0.2


def norm_rows(source, gain):
    wide = source.astype(jnp.float32)
    return wide * lax.rsqrt(jnp.mean(wide * wide, axis=-1, keepdims=True) + epsilon) * gain


def mixed_weights(scores, own_scores, mix_lambda):
    peak = jnp.maximum(jnp.max(scores, axis=-1), own_scores)
    weights = jnp.exp(scores - peak[..., None])
    own_weight = jnp.exp(own_scores - peak)
    denominator = jnp.sum(weights, axis=-1) + own_weight
    shares = weights / denominator[..., None]
    own_share = own_weight / denominator
    balance = mix_lambda[None, :]
    mix_weights = (shares[:, :, 0] - balance[..., None] * shares[:, :, 1]).astype(jnp.bfloat16)
    own_mixed = (own_share[:, :, 0] - balance * own_share[:, :, 1]).astype(jnp.bfloat16)
    return (mix_weights, own_mixed)


def per_device(
    tokens,
    lengths,
    key_cache,
    value_cache,
    attn_gain,
    w_query,
    w_key,
    w_value,
    mix_lambda,
    head_gain,
    w_out,
    ffn_gain,
    w_gate,
    w_up,
    w_down,
    routes,
    route_weights,
):
    seq_dev, model_width = tokens.shape
    group_heads = w_query.shape[1]
    head_width = w_query.shape[2]
    half_width = head_width // 2
    columns = group_heads * head_width
    cache_len = key_cache.shape[1]
    normed = norm_rows(tokens, attn_gain).astype(jnp.bfloat16)
    queries = (
        jnp.dot(normed, w_query.reshape(model_width, columns), preferred_element_type=jnp.float32)
        .astype(jnp.bfloat16)
        .reshape(seq_dev, group_heads, head_width)
    )
    key_new = (
        jnp.dot(normed, w_key.reshape(model_width, columns), preferred_element_type=jnp.float32)
        .astype(jnp.bfloat16)
        .reshape(seq_dev, group_heads, head_width)
    )
    value_new = (
        jnp.dot(normed, w_value.reshape(model_width, columns), preferred_element_type=jnp.float32)
        .astype(jnp.bfloat16)
        .reshape(seq_dev, group_heads, head_width)
    )
    halves = (lax.iota(jnp.int32, head_width) < half_width).astype(jnp.bfloat16)
    stacked_query = jnp.stack([queries * halves, queries * (1 - halves)], axis=2)
    score_scale = half_width ** (-0.5)
    own_scores = (
        jnp.einsum("shcd,shd->shc", stacked_query, key_new, preferred_element_type=jnp.float32)
        * score_scale
    )
    positions = lax.iota(jnp.int32, cache_len)
    live_mask = (positions[None, :] < lengths[:, None])[:, None, None, :]
    scores = (
        jnp.einsum("shcd,slhd->shcl", stacked_query, key_cache, preferred_element_type=jnp.float32)
        * score_scale
    )
    scores = jnp.where(live_mask, scores, -jnp.inf)
    mix_weights, own_mixed = mixed_weights(scores, own_scores, mix_lambda)
    heads_out = jnp.einsum(
        "shl,slhd->shd", mix_weights, value_cache, preferred_element_type=jnp.float32
    )
    heads_out = heads_out + own_mixed.astype(jnp.float32)[..., None] * value_new.astype(jnp.float32)
    normed_heads = (
        heads_out
        * lax.rsqrt(jnp.mean(heads_out * heads_out, axis=-1, keepdims=True) + epsilon)
        * head_gain
        * branch_scale
    ).astype(jnp.bfloat16)
    partial_value = jnp.dot(
        normed_heads.reshape(seq_dev, columns),
        w_out.reshape(columns, model_width),
        preferred_element_type=jnp.float32,
    )
    partial_value = lax.optimization_barrier(partial_value.astype(jnp.bfloat16)).astype(jnp.float32)
    attention = lax.psum(partial_value.astype(jnp.bfloat16), "tp").astype(jnp.float32)
    residual = (tokens.astype(jnp.float32) + attention).astype(jnp.bfloat16)
    normed_ffn = norm_rows(residual, ffn_gain).astype(jnp.bfloat16)
    experts = lax.axis_size("ep")
    top_count = routes.shape[1]
    capacity = 2 * seq_dev * top_count // experts
    entries = routes.reshape(-1)
    onehot = (entries[:, None] == lax.iota(jnp.int32, experts)[None, :]).astype(jnp.int32)
    entry_slot = jnp.sum((jnp.cumsum(onehot, axis=0) - onehot) * onehot, axis=-1)
    target = entries * capacity + entry_slot
    slot_ids = lax.iota(jnp.int32, experts * capacity)
    placing = (slot_ids[:, None] == target[None, :]).astype(jnp.bfloat16)
    repeated = jnp.repeat(normed_ffn, top_count, axis=0)
    outgoing = jnp.dot(placing, repeated, preferred_element_type=jnp.float32).astype(jnp.bfloat16)
    outgoing = outgoing.reshape(experts, capacity, model_width)
    block_cols = model_width // lax.axis_size("tp")
    own_block = lax.dynamic_slice_in_dim(outgoing, lax.axis_index("tp") * block_cols, block_cols, 2)
    arrived = lax.all_gather(
        lax.all_to_all(own_block, "ep", split_axis=0, concat_axis=0, tiled=True),
        "tp",
        axis=2,
        tiled=True,
    )
    sources, slot_count, _ = arrived.shape
    flat_rows = arrived.reshape(sources * slot_count, model_width)
    gate_value = jnp.minimum(
        jnp.dot(flat_rows, w_gate[0], preferred_element_type=jnp.float32), clamp_limit
    )
    up_value = jnp.clip(
        jnp.dot(flat_rows, w_up[0], preferred_element_type=jnp.float32), -clamp_limit, clamp_limit
    )
    activated = ((up_value + 1.0) * gate_value * jax.nn.sigmoid(sigmoid_slope * gate_value)).astype(
        jnp.bfloat16
    )
    pieces = jnp.dot(activated, w_down[0], preferred_element_type=jnp.float32)
    pieces = lax.optimization_barrier(pieces.astype(jnp.bfloat16)).astype(jnp.float32)
    summed = lax.psum_scatter(
        pieces.reshape(sources, slot_count, model_width).astype(jnp.bfloat16),
        "tp",
        scatter_dimension=2,
        tiled=True,
    )
    returned = lax.all_to_all(summed, "ep", split_axis=0, concat_axis=0, tiled=True)
    slice_width = returned.shape[2]
    returned = returned.reshape(experts * capacity, slice_width).astype(jnp.float32)
    chosen = (target.reshape(seq_dev, top_count)[..., None] == slot_ids[None, None, :]).astype(
        jnp.float32
    )
    combine = jnp.sum(route_weights[..., None] * chosen, axis=1)
    expert_sum = jnp.dot(combine, returned, precision=lax.Precision.HIGHEST)
    own_columns = lax.dynamic_slice_in_dim(
        residual, lax.axis_index("tp") * slice_width, slice_width, 1
    )
    return (own_columns.astype(jnp.float32) + expert_sum).astype(jnp.bfloat16)


def solution(mesh):
    placed = (
        P("ep", None),
        P("ep"),
        P("ep", None, "tp", None),
        P("ep", None, "tp", None),
        P(),
        P(None, "tp", None),
        P(None, "tp", None),
        P(None, "tp", None),
        P("tp"),
        P(),
        P("tp", None, None),
        P(),
        P("ep", None, "tp"),
        P("ep", None, "tp"),
        P("ep", "tp", None),
        P("ep", None),
        P("ep", None),
    )
    return jax.shard_map(
        per_device, mesh=mesh, in_specs=placed, out_specs=P("ep", "tp"), check_vma=False
    )
```

profile of v0, /device:TPU:0, one launch (start us, length us, event | category | flops | bytes accessed | tf_op | source)
XLA Modules:
  0.0 125.2 jit_solution(6556066839307545895)
XLA Ops:
  6.6 1.1 fusion.55
  7.7 1.6 %convolution_convert_fusion.4 = bf16[16,256]{1,0:T(8,128)(2,1)S(1)} fusion(bf16[256,8,2,128]{3,2,1,0:T(2,128)(2,1)} %bitcast.110, bf16[16,2048]{1,0:T(8,128)(2,1)} %param.17, f32[2048]{0:T(1024)} %param.21, f32[16]{0:T(128)S(1)} %add_rsqrt_fusion.2), kind=kOutput, calls=%fused_computation.26 | convolution fusion | flops 16912384 | bytes 1130560 | tf_op jit(solution)/shard_map/dot_general | solution.py:57
  9.3 1.6 %convolution_convert_fusion.3 = bf16[16,256]{1,0:T(8,128)(2,1)S(1)} fusion(bf16[256,8,2,128]{3,2,1,0:T(2,128)(2,1)} %bitcast.111, bf16[16,2048]{1,0:T(8,128)(2,1)} %param.17, f32[2048]{0:T(1024)} %param.21, f32[16]{0:T(128)S(1)} %add_rsqrt_fusion.2), kind=kOutput, calls=%fused_computation.25 | convolution fusion | flops 16912384 | bytes 1130560 | tf_op jit(solution)/shard_map/dot_general | solution.py:62
  11.0 0.1 fusion.90
  11.1 0.1 copy.68
  11.3 5.8 %fusion.89 = (f32[16,2,2]{2,1,0:T(2,128)S(1)}, f32[16,2,2,1024]{3,2,1,0:T(2,128)S(1)}) fusion(bf16[16,2,2,128]{3,2,1,0:T(2,128)(2,1)S(1)} %pad_maximum_fusion, bf16[16,1024,2,128]{3,2,1,0:T(2,128)(2,1)} %param.19, pred[16,1024]{1,0:T(8,128)(4,1)S(1)} %iota_compare_fusion.1), kind=kOutput, calls=%fused_computation.105 | convolution fusion | flops 16973760 | bytes 8683776 | tf_op jit(solution)/shard_map/shcd,slhd->shcl/dot_general | solution.py:81
  17.2 0.1 copy.59
  17.3 0.1 copy.60
  17.4 0.3 fusion.51
  17.7 0.1 copy.61
  17.8 0.1 copy.62
  17.9 0.3 fusion.50
  18.2 0.2 fusion.88
  18.5 0.3 fusion.35
  18.8 0.2 fusion.66
  19.1 4.8 %fusion = f32[16,2,1,128]{3,2,1,0:T(1,128)S(1)} fusion(bf16[16,1024,2,128]{3,2,1,0:T(2,128)(2,1)} %param.20, bf16[16,2,1024,1]{2,1,0,3:T(2,128)(2,1)S(1)} %fusion.66), kind=kOutput, calls=%fused_computation | convolution fusion | flops 8388608 | bytes 8470528 | tf_op jit(solution)/shard_map/shl,slhd->shd/dot_general | solution.py:86
  23.9 0.2 multiply_reduce_fusion
  24.1 0.9 fusion.4
  25.3 0.1 reduce_window_sum.11
  25.4 0.2 select_reduce_fusion.1
  25.6 33.8 %all-reduce.2.cloned.1.call-done = bf16[16,2048]{1,0:T(8,128)(2,1)} async-done(((bf16[16,2048]{1,0:T(8,128)(2,1)}), bf16[16,2048]{1,0:T(8,128)(2,1)}) %all-reduce.2.cloned.1.call-update) | async-done | bytes 65552 | tf_op jit(solution)/shard_map/psum | solution.py:102
  59.4 1.0 fusion.52
  60.5 0.1 broadcast_in_dim.16
  60.7 0.3 convolution_convert_fusion.1
  61.0 12.7 %all_to_all.10 = bf16[8,16,512]{2,1,0:T(8,128)(2,1)S(1)} all-to-all(bf16[8,16,512]{2,1,0:T(8,128)(2,1)S(1)} %constant_dynamic-slice_fusion), channel_id=1, replica_groups=mesh['ep'=8,'tp'=4] {'ep'}, dimensions={0} | all-to-all | bytes 262144 | tf_op jit(solution)/shard_map/all_to_all | solution.py:120
  73.6 6.5 %all_gather.3 = bf16[8,16,2048]{2,1,0:T(8,128)(2,1)S(1)} all-gather(bf16[8,16,512]{2,1,0:T(8,128)(2,1)S(1)} %all_to_all.10), channel_id=1, replica_groups=mesh['ep'=8,'tp'=4] {'tp'}, dimensions={2}, use_global_device_ids=true | all-gather | bytes 655360 | tf_op jit(solution)/shard_map/all_gather | solution.py:119
  80.1 2.0 %fusion.13 = f32[128,512]{1,0:T(8,128)S(1)} fusion(bf16[128,2048]{1,0:T(8,128)(2,1)S(1)} %bitcast.105, bf16[1,2048,512]{2,1,0:T(8,128)(2,1)} %param.29), kind=kOutput, calls=%fused_computation.14 | convolution fusion | flops 268500992 | bytes 2883584 | tf_op jit(solution)/shard_map/dot_general | solution.py:128
  82.2 3.2 %convolution_convert_fusion = bf16[128,2048]{1,0:T(8,128)(2,1)} fusion(bf16[1,512,2048]{2,1,0:T(8,128)(2,1)S(1)} %copy-done, f32[128,512]{1,0:T(8,128)S(1)} %fusion.13, bf16[128,2048]{1,0:T(8,128)(2,1)S(1)} %bitcast.106, bf16[1,2048,512]{2,1,0:T(8,128)(2,1)} %param.30), kind=kOutput, calls=%fused_computation.4 | convolution fusion | flops 537722880 | bytes 5505024 | tf_op jit(solution)/shard_map/dot_general | solution.py:136
  85.6 19.2 %reduce-scatter.2.cloned.1.call-done = bf16[8,16,512]{2,1,0:T(8,128)(2,1)} async-done(((bf16[8,16,2048]{2,1,0:T(8,128)(2,1)}), bf16[8,16,512]{2,1,0:T(8,128)(2,1)}) %reduce-scatter.2.cloned.1.call-update) | async-done | bytes 131088 | tf_op jit(solution)/shard_map/reduce_scatter | solution.py:138
  104.8 5.5 %all-to-all-start.1 = ((bf16[8,16,512]{2,1,0:T(8,128)(2,1)}), bf16[8,16,512]{2,1,0:T(8,128)(2,1)S(1)}, u32[]{:S(2)}, u32[]{:S(2)}) async-start(bf16[8,16,512]{2,1,0:T(8,128)(2,1)} %reduce-scatter.2.cloned.1.call-done), calls=%async_computation.2 | async-start | bytes 262144 | tf_op jit(solution)/shard_map/all_to_all | solution.py:144
  110.4 7.2 %all-to-all-done.1 = bf16[8,16,512]{2,1,0:T(8,128)(2,1)S(1)} async-done(((bf16[8,16,512]{2,1,0:T(8,128)(2,1)}), bf16[8,16,512]{2,1,0:T(8,128)(2,1)S(1)}, u32[]{:S(2)}, u32[]{:S(2)}) %all-to-all-start.1) | async-done | bytes 131104 | tf_op jit(solution)/shard_map/all_to_all | solution.py:144
  117.6 0.8 fusion.33
  (50 shorter events, 1.1 us)
Async XLA Ops:
  6.5 75.6 %copy-start = (bf16[1,512,2048]{2,1,0:T(8,128)(2,1)S(1)}, bf16[1,512,2048]{2,1,0:T(8,128)(2,1)}, u32[]{:S(2)}) copy-start(bf16[1,512,2048]{2,1,0:T(8,128)(2,1)} %param.31) | copy-start | bytes 6291460
  6.5 4.7 %copy-start.8 = (s32[16]{0:T(128)S(1)}, s32[16]{0:T(128)}, u32[]{:S(2)}) copy-start(s32[16]{0:T(128)} %param.18) | copy-start | bytes 196
  6.5 52.9 %all-reduce.2.cloned.1.call-start = ((), (), s32[]{:S(2)}) async-start(), calls=%async_computation.3 | async-start | bytes 131072 | tf_op jit(solution)/shard_map/psum | solution.py:102
  11.3 7.2 %copy-start.2 = (bf16[16,2048]{1,0:T(8,128)(2,1)S(1)}, bf16[16,2048]{1,0:T(8,128)(2,1)}, u32[]{:S(2)}) copy-start(bf16[16,2048]{1,0:T(8,128)(2,1)} %param.17) | copy-start | bytes 196612
  11.3 7.2 %copy-start.9 = (bf16[2048,2,128]{2,1,0:T(2,128)(2,1)S(1)}, bf16[2048,2,128]{2,1,0:T(2,128)(2,1)}, u32[]{:S(2)}) copy-start(bf16[2048,2,128]{2,1,0:T(2,128)(2,1)} %param.24) | copy-start | bytes 3145732
  11.3 7.2 %copy-start.10 = (f32[2048]{0:T(1024)S(1)}, f32[2048]{0:T(1024)}, u32[]{:S(2)}) copy-start(f32[2048]{0:T(1024)} %param.21) | copy-start | bytes 24580
  17.2 1.6 %copy-start.5 = (f32[2]{0:T(128)S(1)}, f32[2]{0:T(128)}, u32[]{:S(2)}) copy-start(f32[2]{0:T(128)} %param.25) | copy-start | bytes 28
  19.0 5.0 %copy-start.1 = (bf16[2,128,2048]{2,1,0:T(8,128)(2,1)S(1)}, bf16[2,128,2048]{2,1,0:T(8,128)(2,1)}, u32[]{:S(2)}) copy-start(bf16[2,128,2048]{2,1,0:T(8,128)(2,1)} %param.27) | copy-start | bytes 3145732
  19.0 5.0 %copy-start.7 = (f32[128]{0:T(128)S(1)}, f32[128]{0:T(128)}, u32[]{:S(2)}) copy-start(f32[128]{0:T(128)} %param.26) | copy-start | bytes 1540
  19.0 6.0 %copy-start.4 = (s32[16,4]{0,1:T(4,128)S(1)}, s32[16,4]{0,1:T(4,128)}, u32[]{:S(2)}) copy-start(s32[16,4]{0,1:T(4,128)} %param.32) | copy-start | bytes 772
  19.1 41.3 %copy-start.3 = (f32[2048]{0:T(1024)S(1)}, f32[2048]{0:T(1024)}, u32[]{:S(2)}) copy-start(f32[2048]{0:T(1024)} %param.28) | copy-start | bytes 24580
  25.0 79.8 %reduce-scatter.2.cloned.1.call-start = ((), (), s32[]{:S(2)}) async-start(), calls=%async_computation.4 | async-start | bytes 655360 | tf_op jit(solution)/shard_map/reduce_scatter | solution.py:138
  82.2 28.1 %copy-start.6 = (f32[16,4]{0,1:T(4,128)S(1)}, f32[16,4]{0,1:T(4,128)}, u32[]{:S(2)}) copy-start(f32[16,4]{0,1:T(4,128)} %param.33) | copy-start | bytes 772
  104.8 12.8 %all-to-all-start.1 = ((bf16[8,16,512]{2,1,0:T(8,128)(2,1)}), bf16[8,16,512]{2,1,0:T(8,128)(2,1)S(1)}, u32[]{:S(2)}, u32[]{:S(2)}) async-start(bf16[8,16,512]{2,1,0:T(8,128)(2,1)} %reduce-scatter.2.cloned.1.call-done), calls=%async_computation.2 | async-start | bytes 262144 | tf_op jit(solution)/shard_map/all_to_all | solution.py:144
Sparse Core Ops, SparseCore 0:
  25.1 34.2 all-reduce.1
  85.6 19.1 reduce-scatter.1
where the time goes:
time: 126 us; the launch traced here: 125 us
  waiting for transfers between devices  60.2 us (48%)
  matrix products  21.5 us (17%)
  blocking collectives  19.1 us (15%)
  between operations  13.7 us (11%)
  starting transfers between devices  5.55 us (4%)
  other arithmetic  3.87 us (3%)
  local copies, waits for them, and re-layouts  1.29 us (1%)
    psum x1, waiting for transfers between devices, per_device(): lax.psum(partial_value.astype(jnp.bfloat16), 'tp').astype(jnp.float32)  33.8 us
    reduce_scatter x1, waiting for transfers between devices, per_device(): lax.psum_scatter(pieces.reshape(sources, slot_count, model_width).astype(...  19.2 us
    all_to_all x1, blocking collectives, per_device(): lax.all_to_all(own_block, 'ep', split_axis=0, concat_axis=0, tiled=True)  12.7 us
    all_to_all x1, waiting for transfers between devices, per_device(): lax.all_to_all(summed, 'ep', split_axis=0, concat_axis=0, tiled=True)  7.24 us
    all_gather x1, blocking collectives, per_device(): lax.all_gather(lax.all_to_all(own_block, 'ep', split_axis=0, concat_axis=...  6.49 us
    dot_general x1, matrix products, per_device(): jnp.einsum('shcd,slhd->shcl', stacked_query, key_cache, preferred_element...  5.84 us
    all_to_all x1, starting transfers between devices, per_device(): lax.all_to_all(summed, 'ep', split_axis=0, concat_axis=0, tiled=True)  5.5 us
    dot_general x1, matrix products, per_device(): jnp.einsum('shl,slhd->shd', mix_weights, value_cache, preferred_element_t...  4.8 us
  transfers between devices with their start and end apart: 3, of which 3 were waited for; matrix products, arithmetic and copies ran while one was open for 1% of the time, Pallas kernels for 0%

commit v1 on v0

--- a/solution.py
+++ b/solution.py
@@ -98,83 +98,112 @@
         w_out.reshape(columns, model_width),
         preferred_element_type=jnp.float32,
     )
-    partial_value = lax.optimization_barrier(partial_value.astype(jnp.bfloat16)).astype(jnp.float32)
-    attention = lax.psum(partial_value.astype(jnp.bfloat16), "tp").astype(jnp.float32)
-    residual = (tokens.astype(jnp.float32) + attention).astype(jnp.bfloat16)
-    normed_ffn = norm_rows(residual, ffn_gain).astype(jnp.bfloat16)
+    partial_value = partial_value.astype(jnp.bfloat16)
+    own_core = lax.axis_index("core")
+    rows_y = lax.axis_size("y")
+    width = model_width // (2 * rows_y)
     experts = lax.axis_size("ep")
     top_count = routes.shape[1]
-    capacity = 2 * seq_dev * top_count // experts
-    entries = routes.reshape(-1)
-    onehot = (entries[:, None] == lax.iota(jnp.int32, experts)[None, :]).astype(jnp.int32)
-    entry_slot = jnp.sum((jnp.cumsum(onehot, axis=0) - onehot) * onehot, axis=-1)
-    target = entries * capacity + entry_slot
-    slot_ids = lax.iota(jnp.int32, experts * capacity)
-    placing = (slot_ids[:, None] == target[None, :]).astype(jnp.bfloat16)
-    repeated = jnp.repeat(normed_ffn, top_count, axis=0)
-    outgoing = jnp.dot(placing, repeated, preferred_element_type=jnp.float32).astype(jnp.bfloat16)
-    outgoing = outgoing.reshape(experts, capacity, model_width)
-    block_cols = model_width // lax.axis_size("tp")
-    own_block = lax.dynamic_slice_in_dim(outgoing, lax.axis_index("tp") * block_cols, block_cols, 2)
-    arrived = lax.all_gather(
-        lax.all_to_all(own_block, "ep", split_axis=0, concat_axis=0, tiled=True),
-        "tp",
-        axis=2,
-        tiled=True,
-    )
-    sources, slot_count, _ = arrived.shape
-    flat_rows = arrived.reshape(sources * slot_count, model_width)
+    capacity = min(seq_dev, 2 * seq_dev * top_count // experts)
+
+    def halves_of(source):
+        blocks = source.reshape(source.shape[0], rows_y, 2, width)
+        kept = lax.dynamic_index_in_dim(blocks, own_core, 2, keepdims=False)
+        sent = lax.dynamic_index_in_dim(blocks, 1 - own_core, 2, keepdims=False)
+        return kept, sent
+
+    def swap_cores(source):
+        return lax.ppermute(source, "core", [(0, 1), (1, 0)])
+
+    def pair_sum(source):
+        kept, sent = halves_of(source)
+        arrived = swap_cores(sent)
+        return (kept.astype(jnp.float32) + arrived.astype(jnp.float32)).astype(jnp.bfloat16)
+
+    pair = pair_sum(partial_value)
+    if rows_y == 2:
+        other = lax.ppermute(pair, "y", [(0, 1), (1, 0)])
+        attention = pair.astype(jnp.float32) + other.astype(jnp.float32)
+    else:
+        attention = jnp.sum(lax.all_gather(pair, "y").astype(jnp.float32), axis=0)
+    own_tokens, _ = halves_of(tokens)
+    residual = (own_tokens.astype(jnp.float32) + attention).astype(jnp.bfloat16)
+    half_width_all = rows_y * width
+    flat_residual = residual.reshape(seq_dev, half_width_all)
+    if capacity < seq_dev:
+        entries = routes.reshape(-1)
+        onehot = (entries[:, None] == lax.iota(jnp.int32, experts)[None, :]).astype(jnp.int32)
+        entry_slot = jnp.sum((jnp.cumsum(onehot, axis=0) - onehot) * onehot, axis=-1)
+        target = (entries * capacity + entry_slot).reshape(seq_dev, top_count)
+        slot_ids = lax.iota(jnp.int32, experts * capacity)
+        chosen = (target[..., None] == slot_ids[None, None, :]).astype(jnp.float32)
+        placing = jnp.sum(chosen, axis=1).astype(jnp.bfloat16)
+        outgoing = lax.dot_general(
+            placing, flat_residual, (((0,), (0,)), ((), ())), preferred_element_type=jnp.float32
+        ).astype(jnp.bfloat16)
+        outgoing = outgoing.reshape(experts, capacity, half_width_all)
+    else:
+        outgoing = jnp.broadcast_to(flat_residual[None], (experts, seq_dev, half_width_all))
+    arrived = lax.all_to_all(outgoing, "ep", split_axis=0, concat_axis=0, tiled=True)
+    own_half = arrived.reshape(experts * capacity, rows_y, width)
+    other_half = swap_cores(own_half)
+    flat_rows = jnp.where(
+        own_core == 0,
+        jnp.stack([own_half, other_half], axis=2),
+        jnp.stack([other_half, own_half], axis=2),
+    ).reshape(experts * capacity, model_width)
+    normed_ffn = norm_rows(flat_rows, ffn_gain).astype(jnp.bfloat16)
     gate_value = jnp.minimum(
-        jnp.dot(flat_rows, w_gate[0], preferred_element_type=jnp.float32), clamp_limit
+        jnp.dot(normed_ffn, w_gate[0], preferred_element_type=jnp.float32), clamp_limit
     )
     up_value = jnp.clip(
-        jnp.dot(flat_rows, w_up[0], preferred_element_type=jnp.float32), -clamp_limit, clamp_limit
+        jnp.dot(normed_ffn, w_up[0], preferred_element_type=jnp.float32), -clamp_limit, clamp_limit
     )
     activated = ((up_value + 1.0) * gate_value * jax.nn.sigmoid(sigmoid_slope * gate_value)).astype(
         jnp.bfloat16
     )
-    pieces = jnp.dot(activated, w_down[0], preferred_element_type=jnp.float32)
-    pieces = lax.optimization_barrier(pieces.astype(jnp.bfloat16)).astype(jnp.float32)
-    summed = lax.psum_scatter(
-        pieces.reshape(sources, slot_count, model_width).astype(jnp.bfloat16),
-        "tp",
-        scatter_dimension=2,
-        tiled=True,
-    )
-    returned = lax.all_to_all(summed, "ep", split_axis=0, concat_axis=0, tiled=True)
-    slice_width = returned.shape[2]
-    returned = returned.reshape(experts * capacity, slice_width).astype(jnp.float32)
-    chosen = (target.reshape(seq_dev, top_count)[..., None] == slot_ids[None, None, :]).astype(
-        jnp.float32
-    )
-    combine = jnp.sum(route_weights[..., None] * chosen, axis=1)
-    expert_sum = jnp.dot(combine, returned, precision=lax.Precision.HIGHEST)
-    own_columns = lax.dynamic_slice_in_dim(
-        residual, lax.axis_index("tp") * slice_width, slice_width, 1
-    )
+    pieces = jnp.dot(activated, w_down[0], preferred_element_type=jnp.float32).astype(jnp.bfloat16)
+    pieces = pair_sum(pieces).reshape(experts, capacity, rows_y, width)
+    pieces = pieces.transpose(0, 2, 1, 3).reshape(experts * rows_y, capacity, width)
+    returned = lax.all_to_all(pieces, ("ep", "y"), split_axis=0, concat_axis=0, tiled=True)
+    returned = returned.reshape(experts, rows_y, capacity, width).astype(jnp.float32)
+    expert_out = jnp.sum(returned, axis=1).astype(jnp.bfloat16).astype(jnp.float32)
+    if capacity < seq_dev:
+        combine = jnp.sum(route_weights[..., None] * chosen, axis=1)
+        expert_sum = jnp.dot(
+            combine, expert_out.reshape(experts * capacity, width), precision=lax.Precision.HIGHEST
+        )
+    else:
+        named = routes[..., None] == lax.iota(jnp.int32, experts)[None, None, :]
+        weights = jnp.sum(jnp.where(named, route_weights[..., None], 0.0), axis=1)
+        expert_sum = jnp.sum(weights.T[:, :, None] * expert_out, axis=0)
+    own_columns = lax.dynamic_index_in_dim(residual, lax.axis_index("y"), 1, keepdims=False)
     return (own_columns.astype(jnp.float32) + expert_sum).astype(jnp.bfloat16)
 
 
 def solution(mesh):
+    experts, shards = mesh.shape["ep"], mesh.shape["tp"]
+    split = jax.sharding.Mesh(mesh.devices.reshape(experts, shards // 2, 2), ("ep", "y", "core"))
+    tp = ("y", "core")
     placed = (
         P("ep", None),
         P("ep"),
-        P("ep", None, "tp", None),
-        P("ep", None, "tp", None),
+        P("ep", None, tp, None),
+        P("ep", None, tp, None),
         P(),
-        P(None, "tp", None),
-        P(None, "tp", None),
-        P(None, "tp", None),
-        P("tp"),
+        P(None, tp, None),
+        P(None, tp, None),
+        P(None, tp, None),
+        P(tp),
         P(),
-        P("tp", None, None),
+        P(tp, None, None),
         P(),
-        P("ep", None, "tp"),
-        P("ep", None, "tp"),
-        P("ep", "tp", None),
+        P("ep", None, tp),
+        P("ep", None, tp),
+        P("ep", tp, None),
         P("ep", None),
         P("ep", None),
     )
     return jax.shard_map(
-        per_device, mesh=mesh, in_specs=placed, out_specs=P("ep", "tp"), check_vma=False
-    )
+        per_device, mesh=split, in_specs=placed, out_specs=P("ep", tp), check_vma=False
+    )

time: 126 us -> 65.6 us (0.52)
  waiting for transfers between devices: 60.2 us -> 15.4 us
  between operations: 13.7 us -> 0.38 us
  blocking collectives: 19.1 us -> 14.3 us
  local copies, waits for them, and re-layouts: 1.29 us -> 4.05 us
  starting transfers between devices: 5.55 us -> 8.25 us
  matrix products: 21.5 us -> 19 us
    psum x1 -> x0, waiting for transfers between devices: 33.8 us -> none  [per_device(): lax.psum(partial_value.astype(jnp.bfloat16), 'tp').astype(jnp.float32)]
    reduce_scatter x1 -> x0, waiting for transfers between devices: 19.2 us -> none  [per_device(): lax.psum_scatter(pieces.reshape(sources, slot_count, model_width).astype(...]
    all_gather x1 -> x0, blocking collectives: 6.49 us -> none  [per_device(): lax.all_gather(lax.all_to_all(own_block, 'ep', split_axis=0, concat_axis=...]
    ppermute x0 -> x4, waiting for transfers between devices: none -> 5.31 us  [the longest x3 3.49 us: swap_cores(): return lax.ppermute(source, 'core', [(0, 1), (1, 0)])]
    ppermute x0 -> x4, starting transfers between devices: none -> 3.75 us  [the longest x1 2.92 us: per_device(): other = lax.ppermute(pair, 'y', [(0, 1), (1, 0)])]
    all_to_all x1, waiting for transfers between devices: 7.24 us -> 10.1 us  [per_device(): lax.all_to_all(pieces, ('ep', 'y'), split_axis=0, concat_axis=0, tiled=True)]
    dot_general x4 -> x2, matrix products: 6.33 us -> 4.53 us  [the longest x1 2.46 us: per_device(): jnp.dot(activated, w_down[0], preferred_element_type=jnp.float32)]
    all_to_all x1, blocking collectives: 12.7 us -> 14.3 us  [per_device(): lax.all_to_all(outgoing, 'ep', split_axis=0, concat_axis=0, tiled=True)]
  transfers between devices with their start and end apart: 3 -> 5, of which waited for: 3 -> 5; matrix products, arithmetic and copies ran while one was open for 1% -> 1% of each run, Pallas kernels for 0% -> 0%
where the time goes in v1:
time: 65.6 us; the launch traced here: 65.2 us
  matrix products  19 us (29%)
  waiting for transfers between devices  15.4 us (23%)
  blocking collectives  14.3 us (22%)
  starting transfers between devices  8.25 us (13%)
  local copies, waits for them, and re-layouts  4.05 us (6%)
  other arithmetic  3.7 us (6%)
    all_to_all x1, blocking collectives, per_device(): lax.all_to_all(outgoing, 'ep', split_axis=0, concat_axis=0, tiled=True)  14.3 us
    all_to_all x1, waiting for transfers between devices, per_device(): lax.all_to_all(pieces, ('ep', 'y'), split_axis=0, concat_axis=0, tiled=True)  10.1 us
    dot_general x1, matrix products, per_device(): jnp.einsum('shcd,slhd->shcl', stacked_query, key_cache, preferred_element...  5.84 us
    dot_general x1, matrix products, per_device(): jnp.einsum('shl,slhd->shd', mix_weights, value_cache, preferred_element_t...  4.8 us
    all_to_all x1, starting transfers between devices, per_device(): lax.all_to_all(pieces, ('ep', 'y'), split_axis=0, concat_axis=0, tiled=True)  4.5 us
    ppermute x3, waiting for transfers between devices, swap_cores(): return lax.ppermute(source, 'core', [(0, 1), (1, 0)])  3.49 us
    ppermute x1, starting transfers between devices, per_device(): other = lax.ppermute(pair, 'y', [(0, 1), (1, 0)])  2.92 us
    dot_general x1, matrix products, per_device(): jnp.dot(activated, w_down[0], preferred_element_type=jnp.float32)  2.46 us
  transfers between devices with their start and end apart: 5, of which 5 were waited for; matrix products, arithmetic and copies ran while one was open for 1% of the time, Pallas kernels for 0%

profile of v1, /device:TPU:0, one launch (start us, length us, event | category | flops | bytes accessed | tf_op | source)
XLA Modules:
  0.0 65.2 jit_solution(2998511466045371019)
XLA Ops:
  0.0 1.1 %fusion.55 = f32[16]{0:T(128)S(1)} fusion(bf16[16,2048]{1,0:T(8,128)(2,1)} %param.17), kind=kLoop, calls=%fused_computation.54 | loop fusion | flops 98288 | bytes 65600 | tf_op jit(solution)/shard_map/reduce_sum | solution.py:14
  1.1 1.6 %convolution_convert_fusion.3 = bf16[16,256]{1,0:T(8,128)(2,1)S(1)} fusion(bf16[256,8,2,128]{3,2,1,0:T(2,128)(2,1)} %bitcast.145, bf16[16,2048]{1,0:T(8,128)(2,1)} %param.17, f32[2048]{0:T(1024)} %param.21, f32[16]{0:T(128)S(1)} %add_rsqrt_fusion.2), kind=kOutput, calls=%fused_computation.25 | convolution fusion | flops 16912384 | bytes 1130560 | tf_op jit(solution)/shard_map/dot_general | solution.py:57
  2.7 1.6 %convolution_convert_fusion.2 = bf16[16,256]{1,0:T(8,128)(2,1)S(1)} fusion(bf16[256,8,2,128]{3,2,1,0:T(2,128)(2,1)} %bitcast.146, bf16[16,2048]{1,0:T(8,128)(2,1)} %param.17, f32[2048]{0:T(1024)} %param.21, f32[16]{0:T(128)S(1)} %add_rsqrt_fusion.2), kind=kOutput, calls=%fused_computation.24 | convolution fusion | flops 16912384 | bytes 1130560 | tf_op jit(solution)/shard_map/dot_general | solution.py:62
  4.8 5.8 %fusion.88 = (f32[16,2,2]{2,1,0:T(2,128)S(1)}, f32[16,2,2,1024]{3,2,1,0:T(2,128)S(1)}) fusion(bf16[16,2,2,128]{3,2,1,0:T(2,128)(2,1)S(1)} %pad_maximum_fusion, bf16[16,1024,2,128]{3,2,1,0:T(2,128)(2,1)} %param.19, pred[16,1024]{1,0:T(8,128)(4,1)S(1)} %iota_compare_fusion), kind=kOutput, calls=%fused_computation.114 | convolution fusion | flops 16973760 | bytes 8683776 | tf_op jit(solution)/shard_map/shcd,slhd->shcl/dot_general | solution.py:81
  10.8 0.3 fusion.54
  11.4 0.3 fusion.53
  11.7 0.2 fusion.87
  11.9 0.3 fusion.34
  12.5 4.8 %fusion = f32[16,2,1,128]{3,2,1,0:T(1,128)S(1)} fusion(bf16[16,1024,2,128]{3,2,1,0:T(2,128)(2,1)} %param.20, bf16[16,2,1024,1]{2,1,0,3:T(2,128)(2,1)S(1)} %fusion.67), kind=kOutput, calls=%fused_computation | convolution fusion | flops 8388608 | bytes 8470528 | tf_op jit(solution)/shard_map/shl,slhd->shd/dot_general | solution.py:86
  17.3 0.2 multiply_reduce_fusion.1
  17.5 0.3 fusion.4
  18.0 0.6 collective-permute-start
  18.6 0.8 %collective-permute-done = bf16[16,2,512]{2,0,1:T(8,128)(2,1)S(1)} collective-permute-done((bf16[16,2,512]{2,0,1:T(8,128)(2,1)S(1)}, bf16[16,2,512]{2,0,1:T(8,128)(2,1)S(1)}, u32[]{:S(2)}, u32[]{:S(2)}) %collective-permute-start) | collective-permute-done | bytes 32800 | tf_op jit(solution)/shard_map/ppermute | solution.py:116
  19.5 2.9 %collective-permute-start.1 = (bf16[16,2,512]{2,0,1:T(8,128)(2,1)S(1)}, bf16[16,2,512]{2,0,1:T(8,128)(2,1)S(1)}, u32[]{:S(2)}, u32[]{:S(2)}) collective-permute-start(bf16[16,2,512]{2,0,1:T(8,128)(2,1)S(1)} %fusion.65), channel_id=1, source_target_pairs={{0,2},{2,0},{1,3},{3,1},{4,6},{6,4},{5,7},{7,5},{8,10},{10,8},{9,1... | collective-permute-start | bytes 98312 | tf_op jit(solution)/shard_map/ppermute | solution.py:125
  22.5 1.8 %collective-permute-done.1 = bf16[16,2,512]{2,0,1:T(8,128)(2,1)S(1)} collective-permute-done((bf16[16,2,512]{2,0,1:T(8,128)(2,1)S(1)}, bf16[16,2,512]{2,0,1:T(8,128)(2,1)S(1)}, u32[]{:S(2)}, u32[]{:S(2)}) %collective-permute-start.1) | collective-permute-done | bytes 32800 | tf_op jit(solution)/shard_map/ppermute | solution.py:125
  24.3 14.3 %all_to_all.10 = bf16[8,16,1024]{2,1,0:T(8,128)(2,1)S(1)} all-to-all(bf16[8,16,1024]{2,1,0:T(8,128)(2,1)S(1)} %broadcast_in_dim.29), channel_id=1, replica_groups=mesh['ep'=8,'y'=2,'core'=2] {'ep'}, dimensions={0} | all-to-all | bytes 524288 | tf_op jit(solution)/shard_map/all_to_all | solution.py:147
  38.7 0.2 reshape.234
  39.0 0.2 stack_reshape.4
  39.2 1.3 %collective-permute-done.2 = bf16[128,2,512]{2,1,0:T(2,128)(2,1)S(1)} collective-permute-done((bf16[128,2,512]{2,1,0:T(2,128)(2,1)S(1)}, bf16[128,2,512]{2,1,0:T(2,128)(2,1)S(1)}, u32[]{:S(2)}, u32[]{:S(2)}) %collective-permute-start.2) | collective-permute-done | bytes 262176 | tf_op jit(solution)/shard_map/ppermute | solution.py:116
  40.5 0.2 fusion.35
  40.7 0.2 fusion.37
  40.9 0.3 copy.121
  41.2 2.1 %fusion.13 = f32[128,512]{1,0:T(8,128)S(1)} fusion(bf16[128,2048]{0,1:T(8,128)(2,1)S(1)} %bitcast.135, bf16[1,2048,512]{2,1,0:T(8,128)(2,1)} %param.29), kind=kOutput, calls=%fused_computation.15 | convolution fusion | flops 268500992 | bytes 2883584 | tf_op jit(solution)/shard_map/dot_general | solution.py:157
  43.3 2.5 %convolution_convert_fusion = bf16[128,2048]{1,0:T(8,128)(2,1)S(1)} fusion(bf16[1,512,2048]{2,1,0:T(8,128)(2,1)S(1)} %copy-done, f32[128,512]{1,0:T(8,128)S(1)} %fusion.13, bf16[128,2048]{0,1:T(8,128)(2,1)S(1)} %bitcast.136, bf16[1,2048,512]{2,1,0:T(8,128)(2,1)} %param.30), kind=kOutput, calls=%fused_computation.4 | convolution fusion | flops 537722880 | bytes 5505024 | tf_op jit(solution)/shard_map/dot_general | solution.py:165
  45.8 0.4 reshape.235
  46.2 1.1 %constant_dynamic-slice_fusion.1 = (bf16[128,2,1,512]{3,2,1,0:T(2,128)(2,1)S(1)}, bf16[128,2,1,512]{3,2,1,0:T(2,128)(2,1)S(1)}) fusion(bf16[128,2,2,512]{3,2,1,0:T(2,128)(2,1)S(1)} %reshape.235, s32[]{:T(128)S(6)} %select_n.44, s32[]{:T(128)S(6)} %select_n.46), kind=kLoop, calls=%fused_computation.94 | loop fusion | bytes 1048584 | tf_op jit(solution)/shard_map/jit(dynamic_index_in_dim)/dynamic_slice | solution.py:111
  47.4 0.2 collective-permute-start.3
  47.6 1.4 %collective-permute-done.3 = bf16[128,2,512]{2,0,1:T(8,128)(2,1)S(1)} collective-permute-done((bf16[128,2,512]{2,0,1:T(8,128)(2,1)S(1)}, bf16[128,2,512]{2,0,1:T(8,128)(2,1)S(1)}, u32[]{:S(2)}, u32[]{:S(2)}) %collective-permute-start.3) | collective-permute-done | bytes 262176 | tf_op jit(solution)/shard_map/ppermute | solution.py:116
  49.1 0.7 %copy.124 = bf16[8,16,2,512]{3,1,2,0:T(8,128)(2,1)} copy(bf16[8,16,2,512]{3,1,0,2:T(8,128)(2,1)S(1)} %bitcast.139) | data formatting | bytes 524288 | tf_op jit(solution)/shard_map/reshape | solution.py:166
  49.8 4.5 %all-to-all-start.1 = ((bf16[16,16,512]{2,1,0:T(8,128)(2,1)}), bf16[16,16,512]{2,1,0:T(8,128)(2,1)S(1)}, u32[]{:S(2)}, u32[]{:S(2)}) async-start(bf16[16,16,512]{2,1,0:T(8,128)(2,1)} %bitcast.20), calls=%async_computation.1 | async-start | bytes 524288 | tf_op jit(solution)/shard_map/all_to_all | solution.py:168
  54.3 10.1 %all-to-all-done.1 = bf16[16,16,512]{2,1,0:T(8,128)(2,1)S(1)} async-done(((bf16[16,16,512]{2,1,0:T(8,128)(2,1)}), bf16[16,16,512]{2,1,0:T(8,128)(2,1)S(1)}, u32[]{:S(2)}, u32[]{:S(2)}) %all-to-all-start.1) | async-done | bytes 262176 | tf_op jit(solution)/shard_map/all_to_all | solution.py:168
  64.6 0.6 fusion.68
  (60 shorter events, 2.0 us)
Async XLA Ops:
  0.0 43.3 %copy-start = (bf16[1,512,2048]{2,1,0:T(8,128)(2,1)S(1)}, bf16[1,512,2048]{2,1,0:T(8,128)(2,1)}, u32[]{:S(2)}) copy-start(bf16[1,512,2048]{2,1,0:T(8,128)(2,1)} %param.31) | copy-start | bytes 6291460
  0.0 4.7 %copy-start.8 = (s32[16]{0:T(128)S(1)}, s32[16]{0:T(128)}, u32[]{:S(2)}) copy-start(s32[16]{0:T(128)} %param.18) | copy-start | bytes 196
  4.8 7.2 %copy-start.2 = (bf16[16,2048]{1,0:T(8,128)(2,1)S(1)}, bf16[16,2048]{1,0:T(8,128)(2,1)}, u32[]{:S(2)}) copy-start(bf16[16,2048]{1,0:T(8,128)(2,1)} %param.17) | copy-start | bytes 196612
  4.8 7.2 %copy-start.9 = (bf16[2048,2,128]{2,1,0:T(2,128)(2,1)S(1)}, bf16[2048,2,128]{2,1,0:T(2,128)(2,1)}, u32[]{:S(2)}) copy-start(bf16[2048,2,128]{2,1,0:T(2,128)(2,1)} %param.24) | copy-start | bytes 3145732
  4.8 7.2 %copy-start.10 = (f32[2048]{0:T(1024)S(1)}, f32[2048]{0:T(1024)}, u32[]{:S(2)}) copy-start(f32[2048]{0:T(1024)} %param.21) | copy-start | bytes 24580
  10.6 1.6 %copy-start.4 = (f32[2]{0:T(128)S(1)}, f32[2]{0:T(128)}, u32[]{:S(2)}) copy-start(f32[2]{0:T(128)} %param.25) | copy-start | bytes 28
  12.5 5.0 %copy-start.1 = (bf16[2,128,2048]{2,1,0:T(8,128)(2,1)S(1)}, bf16[2,128,2048]{2,1,0:T(8,128)(2,1)}, u32[]{:S(2)}) copy-start(bf16[2,128,2048]{2,1,0:T(8,128)(2,1)} %param.27) | copy-start | bytes 3145732
  12.5 5.0 %copy-start.7 = (f32[128]{0:T(128)S(1)}, f32[128]{0:T(128)}, u32[]{:S(2)}) copy-start(f32[128]{0:T(128)} %param.26) | copy-start | bytes 1540
  17.3 21.6 %copy-start.3 = (f32[2048]{0:T(1024)S(1)}, f32[2048]{0:T(1024)}, u32[]{:S(2)}) copy-start(f32[2048]{0:T(1024)} %param.28) | copy-start | bytes 24580
  18.0 1.4 %collective-permute-start = (bf16[16,2,512]{2,0,1:T(8,128)(2,1)S(1)}, bf16[16,2,512]{2,0,1:T(8,128)(2,1)S(1)}, u32[]{:S(2)}, u32[]{:S(2)}) collective-permute-start(bf16[16,2,512]{2,0,1:T(8,128)(2,1)S(1)} %bitcast.143), channel_id=1, source_target_pairs={{0,1},{1,0},{2,3},{3,2},{4,5},{5,4},{6,7},{7,6},{8,9},{9,8},{10,11... | collective-permute-start | bytes 98312 | tf_op jit(solution)/shard_map/ppermute | solution.py:116
  19.5 4.8 %collective-permute-start.1 = (bf16[16,2,512]{2,0,1:T(8,128)(2,1)S(1)}, bf16[16,2,512]{2,0,1:T(8,128)(2,1)S(1)}, u32[]{:S(2)}, u32[]{:S(2)}) collective-permute-start(bf16[16,2,512]{2,0,1:T(8,128)(2,1)S(1)} %fusion.65), channel_id=1, source_target_pairs={{0,2},{2,0},{1,3},{3,1},{4,6},{6,4},{5,7},{7,5},{8,10},{10,8},{9,1... | collective-permute-start | bytes 98312 | tf_op jit(solution)/shard_map/ppermute | solution.py:125
  38.9 1.6 %collective-permute-start.2 = (bf16[128,2,512]{2,1,0:T(2,128)(2,1)S(1)}, bf16[128,2,512]{2,1,0:T(2,128)(2,1)S(1)}, u32[]{:S(2)}, u32[]{:S(2)}) collective-permute-start(bf16[128,2,512]{2,1,0:T(2,128)(2,1)S(1)} %reshape.234), channel_id=1, source_target_pairs={{0,1},{1,0},{2,3},{3,2},{4,5},{5,4},{6,7},{7,6},{8,9},{9,8},{10,11... | collective-permute-start | bytes 786440 | tf_op jit(solution)/shard_map/ppermute | solution.py:116
  46.1 8.1 %copy-start.5 = (f32[16,4]{0,1:T(4,128)S(1)}, f32[16,4]{0,1:T(4,128)}, u32[]{:S(2)}) copy-start(f32[16,4]{0,1:T(4,128)} %param.33) | copy-start | bytes 772
  46.2 8.1 %copy-start.6 = (s32[16,4]{0,1:T(4,128)S(1)}, s32[16,4]{0,1:T(4,128)}, u32[]{:S(2)}) copy-start(s32[16,4]{0,1:T(4,128)} %param.32) | copy-start | bytes 772
  47.4 1.6 %collective-permute-start.3 = (bf16[128,2,512]{2,0,1:T(8,128)(2,1)S(1)}, bf16[128,2,512]{2,0,1:T(8,128)(2,1)S(1)}, u32[]{:S(2)}, u32[]{:S(2)}) collective-permute-start(bf16[128,2,512]{2,0,1:T(8,128)(2,1)S(1)} %bitcast.140), channel_id=1, source_target_pairs={{0,1},{1,0},{2,3},{3,2},{4,5},{5,4},{6,7},{7,6},{8,9},{9,8},{10,11... | collective-permute-start | bytes 786440 | tf_op jit(solution)/shard_map/ppermute | solution.py:116
  49.8 14.7 %all-to-all-start.1 = ((bf16[16,16,512]{2,1,0:T(8,128)(2,1)}), bf16[16,16,512]{2,1,0:T(8,128)(2,1)S(1)}, u32[]{:S(2)}, u32[]{:S(2)}) async-start(bf16[16,16,512]{2,1,0:T(8,128)(2,1)} %bitcast.20), calls=%async_computation.1 | async-start | bytes 524288 | tf_op jit(solution)/shard_map/all_to_all | solution.py:168

commit v2 on v1

--- a/solution.py
+++ b/solution.py
@@ -1,12 +1,15 @@
 import jax
 import jax.numpy as jnp
 from jax import lax
+from jax.experimental import pallas as pl
+from jax.experimental.pallas import tpu as pltpu
 from jax.sharding import PartitionSpec as P
 
 epsilon = 1e-06
 clamp_limit = 7.0
 sigmoid_slope = 1.702
 branch_scale = 0.2
+group_rows = 8
 
 
 def norm_rows(source, gain):
@@ -14,17 +17,262 @@
     return wide * lax.rsqrt(jnp.mean(wide * wide, axis=-1, keepdims=True) + epsilon) * gain
 
 
-def mixed_weights(scores, own_scores, mix_lambda):
-    peak = jnp.maximum(jnp.max(scores, axis=-1), own_scores)
-    weights = jnp.exp(scores - peak[..., None])
+def attention_kernel(
+    lengths_hbm,
+    lambda_hbm,
+    tokens_hbm,
+    gain_hbm,
+    head_gain_hbm,
+    query_hbm,
+    key_hbm,
+    value_hbm,
+    keys_hbm,
+    values_hbm,
+    out_hbm,
+    kept_ref,
+    sent_ref,
+    lengths_ref,
+    lambda_ref,
+    tokens_ref,
+    gain_ref,
+    head_gain_ref,
+    weights_ref,
+    keys_ref,
+    values_ref,
+    out_ref,
+    wide_ref,
+    query_ref,
+    scores_ref,
+    peak_ref,
+    total_ref,
+    heads_ref,
+    small_sem,
+    large_sem,
+):
+    seqs, positions, head_width = keys_ref.shape
+    model_width = tokens_ref.shape[1]
+    heads = query_hbm.shape[0] // model_width
+    rows_y, width = kept_ref.shape[0], kept_ref.shape[2]
+    lanes = 128
+    rows = seqs * group_rows
+    f32, bf16 = jnp.float32, jnp.bfloat16
+
+    small = [
+        pltpu.make_async_copy(source, target, small_sem.at[i])
+        for i, (source, target) in enumerate(
+            (
+                (tokens_hbm, tokens_ref),
+                (gain_hbm, gain_ref),
+                (lengths_hbm, lengths_ref),
+                (lambda_hbm, lambda_ref),
+                (head_gain_hbm, head_gain_ref),
+            )
+        )
+    ]
+    for copy in small:
+        copy.start()
+    large = [
+        pltpu.make_async_copy(source, target, large_sem.at[i])
+        for i, (source, target) in enumerate(
+            (
+                (query_hbm, weights_ref.at[0]),
+                (key_hbm, weights_ref.at[1]),
+                (value_hbm, weights_ref.at[2]),
+                (keys_hbm, keys_ref),
+                (values_hbm, values_ref),
+                (out_hbm, out_ref),
+            )
+        )
+    ]
+    for copy in large:
+        copy.start()
+    for copy in small:
+        copy.wait()
+    normed = norm_rows(tokens_ref[...], gain_ref[...]).astype(bf16)
+    spread = (
+        lax.broadcasted_iota(jnp.int32, (lanes, heads * lanes), 1) // heads
+        == lax.broadcasted_iota(jnp.int32, (lanes, heads * lanes), 0)
+    ).astype(bf16)
+    lane_head = lax.broadcasted_iota(jnp.int32, (seqs, heads * lanes), 1) % heads
+    for block in range(model_width // lanes):
+        part = jnp.dot(
+            normed[:, block * lanes : (block + 1) * lanes], spread, preferred_element_type=f32
+        )
+        columns = slice(block * heads * lanes, (block + 1) * heads * lanes)
+        for h in range(heads):
+            wide_ref[h * seqs : (h + 1) * seqs, columns] = jnp.where(
+                lane_head == h, part, 0.0
+            ).astype(bf16)
+
+    row_ids = lax.broadcasted_iota(jnp.int32, (rows, heads * seqs), 0)
+    column_ids = lax.broadcasted_iota(jnp.int32, (rows, heads * seqs), 1)
+    placing = (
+        (column_ids % seqs == row_ids // group_rows)
+        & (column_ids // seqs == (row_ids % group_rows) // 2 % heads)
+    ).astype(bf16)
+
+    def project(i):
+        large[i].wait()
+        product = jnp.dot(wide_ref[...], weights_ref[i], preferred_element_type=f32)
+        return jnp.dot(placing, product.astype(bf16), preferred_element_type=f32)
+
+    place = lax.broadcasted_iota(jnp.int32, (rows, head_width), 0) % group_rows
+    lane = lax.broadcasted_iota(jnp.int32, (rows, head_width), 1)
+    own_half = ((lane < head_width // 2) == (place % 2 == 0)) & (place < 2 * heads)
+    queries = jnp.where(own_half, project(0), 0.0) * (head_width // 2) ** (-0.5)
+    query_ref[...] = queries
+    own_scores = jnp.sum(queries * project(1), axis=-1, keepdims=True)
+    value_new = project(2)
+
+    group = lax.broadcasted_iota(jnp.int32, (group_rows, positions), 0)
+    spot = lax.broadcasted_iota(jnp.int32, (group_rows, positions), 1)
+    own_head = spot % heads == group // 2 % heads
+    spot = jnp.where(own_head, spot, positions)
+
+    def folded(source, combine):
+        parts = [source[:, i : i + lanes] for i in range(0, positions, lanes)]
+        while len(parts) > 1:
+            parts = [combine(a, b) for a, b in zip(parts[::2], parts[1::2])]
+        return parts[0]
+
+    large[3].wait()
+    for s in range(seqs):
+        at = slice(s * group_rows, (s + 1) * group_rows)
+        scores = lax.dot_general(
+            query_ref[at, :].astype(bf16),
+            keys_ref[s],
+            (((1,), (1,)), ((), ())),
+            preferred_element_type=f32,
+        )
+        scores = jnp.where(spot < lengths_ref[s] * heads, scores, -jnp.inf)
+        scores_ref[at, :] = scores
+        peak_ref[at, :] = folded(scores, jnp.maximum)
+
+    peak = jnp.maximum(jnp.max(peak_ref[...], axis=-1, keepdims=True), own_scores)
+    peak_ref[...] = jnp.broadcast_to(peak, peak_ref.shape)
+    for s in range(seqs):
+        at = slice(s * group_rows, (s + 1) * group_rows)
+        shifted = jnp.exp(scores_ref[at, :] - peak_ref[at, 0:1])
+        scores_ref[at, :] = shifted
+        total_ref[at, :] = folded(shifted, jnp.add)
+
     own_weight = jnp.exp(own_scores - peak)
-    denominator = jnp.sum(weights, axis=-1) + own_weight
-    shares = weights / denominator[..., None]
-    own_share = own_weight / denominator
-    balance = mix_lambda[None, :]
-    mix_weights = (shares[:, :, 0] - balance[..., None] * shares[:, :, 1]).astype(jnp.bfloat16)
-    own_mixed = (own_share[:, :, 0] - balance * own_share[:, :, 1]).astype(jnp.bfloat16)
-    return (mix_weights, own_mixed)
+    denominator = jnp.sum(total_ref[...], axis=-1, keepdims=True) + own_weight
+    row = lax.broadcasted_iota(jnp.int32, (rows, 1), 0) % group_rows
+    factor = jnp.ones((rows, 1), f32)
+    for h in range(heads):
+        factor = jnp.where(row == 2 * h + 1, -lambda_ref[h], factor)
+    factor = factor / denominator
+    peak_ref[...] = jnp.broadcast_to(factor, peak_ref.shape)
+    total_ref[...] = jnp.broadcast_to(own_weight * factor, peak_ref.shape)
+    query_ref[...] = value_new
+
+    def mixed(source):
+        return (source + pltpu.roll(source, group_rows - 1, 0)).astype(bf16)
+
+    large[4].wait()
+    for s in range(seqs):
+        at = slice(s * group_rows, (s + 1) * group_rows)
+        weights = mixed(scores_ref[at, :] * peak_ref[at, 0:1])
+        own = mixed(total_ref[at, :]).astype(f32)
+        heads_ref[at, :] = (
+            jnp.dot(weights, values_ref[s], preferred_element_type=f32)
+            + own * query_ref[at, :]
+        )
+
+    heads_out = heads_ref[...]
+    normed_heads = (
+        heads_out
+        * lax.rsqrt(jnp.mean(heads_out * heads_out, axis=-1, keepdims=True) + epsilon)
+        * head_gain_ref[...]
+        * branch_scale
+    ).astype(bf16)
+    picked = []
+    taker = lax.broadcasted_iota(jnp.int32, (seqs, rows), 0) * group_rows
+    giver = lax.broadcasted_iota(jnp.int32, (seqs, rows), 1)
+    for h in range(heads):
+        chosen = (giver == taker + 2 * h).astype(bf16)
+        picked.append(jnp.dot(chosen, normed_heads, preferred_element_type=f32).astype(bf16))
+    joined = jnp.concatenate(picked, axis=1) if heads > 1 else picked[0]
+    large[5].wait()
+    core = lax.axis_index("core")
+    for y in range(rows_y):
+        for target, which in ((sent_ref, 1 - core), (kept_ref, core)):
+            columns = pl.ds(pl.multiple_of((2 * y + which) * width, width), width)
+            target[y] = jnp.dot(
+                joined, out_ref[:, columns], preferred_element_type=f32
+            ).astype(bf16)
+
+
+def attend(
+    tokens,
+    lengths,
+    key_cache,
+    value_cache,
+    attn_gain,
+    w_query,
+    w_key,
+    w_value,
+    mix_lambda,
+    head_gain,
+    w_out,
+    rows_y,
+):
+    seqs, model_width = tokens.shape
+    cache_len, heads, head_width = key_cache.shape[1:]
+    positions = cache_len * heads
+    rows = seqs * group_rows
+    width = model_width // (2 * rows_y)
+    bf16, f32 = jnp.bfloat16, jnp.float32
+    vmem = pl.BlockSpec(memory_space=pltpu.VMEM)
+    hbm = pl.BlockSpec(memory_space=pltpu.HBM)
+    out = jax.ShapeDtypeStruct((rows_y, seqs, width), bf16)
+    return pl.pallas_call(
+        attention_kernel,
+        out_shape=(out, out),
+        in_specs=[hbm] * 11,
+        out_specs=(vmem, vmem),
+        scratch_shapes=[
+            pltpu.SMEM((seqs,), jnp.int32),
+            pltpu.SMEM((heads,), f32),
+            pltpu.VMEM((seqs, model_width), bf16),
+            pltpu.VMEM((1, model_width), f32),
+            pltpu.VMEM((1, head_width), f32),
+            pltpu.VMEM((3, model_width * heads, head_width), bf16),
+            pltpu.VMEM((seqs, positions, head_width), bf16),
+            pltpu.VMEM((seqs, positions, head_width), bf16),
+            pltpu.VMEM((heads * head_width, model_width), bf16),
+            pltpu.VMEM((heads * seqs, heads * model_width), bf16),
+            pltpu.VMEM((rows, head_width), f32),
+            pltpu.VMEM((rows, positions), f32),
+            pltpu.VMEM((rows, 128), f32),
+            pltpu.VMEM((rows, 128), f32),
+            pltpu.VMEM((rows, head_width), f32),
+            pltpu.SemaphoreType.DMA((5,)),
+            pltpu.SemaphoreType.DMA((6,)),
+        ],
+        compiler_params=pltpu.CompilerParams(vmem_limit_bytes=attention_vmem),
+        cost_estimate=pl.CostEstimate(
+            flops=attention_flops, bytes_accessed=4 * key_cache.size, transcendentals=0
+        ),
+        name="attention",
+    )(
+        lengths,
+        mix_lambda,
+        tokens,
+        attn_gain.reshape(1, model_width),
+        head_gain.reshape(1, head_width),
+        w_query.reshape(model_width * heads, head_width),
+        w_key.reshape(model_width * heads, head_width),
+        w_value.reshape(model_width * heads, head_width),
+        key_cache.reshape(seqs, positions, head_width),
+        value_cache.reshape(seqs, positions, head_width),
+        w_out.reshape(heads * head_width, model_width),
+    )
+
+
+attention_vmem = 63 * 1024 * 1024
+attention_flops = 4 * 10**9
 
 
 def per_device(
@@ -47,58 +295,6 @@
     route_weights,
 ):
     seq_dev, model_width = tokens.shape
-    group_heads = w_query.shape[1]
-    head_width = w_query.shape[2]
-    half_width = head_width // 2
-    columns = group_heads * head_width
-    cache_len = key_cache.shape[1]
-    normed = norm_rows(tokens, attn_gain).astype(jnp.bfloat16)
-    queries = (
-        jnp.dot(normed, w_query.reshape(model_width, columns), preferred_element_type=jnp.float32)
-        .astype(jnp.bfloat16)
-        .reshape(seq_dev, group_heads, head_width)
-    )
-    key_new = (
-        jnp.dot(normed, w_key.reshape(model_width, columns), preferred_element_type=jnp.float32)
-        .astype(jnp.bfloat16)
-        .reshape(seq_dev, group_heads, head_width)
-    )
-    value_new = (
-        jnp.dot(normed, w_value.reshape(model_width, columns), preferred_element_type=jnp.float32)
-        .astype(jnp.bfloat16)
-        .reshape(seq_dev, group_heads, head_width)
-    )
-    halves = (lax.iota(jnp.int32, head_width) < half_width).astype(jnp.bfloat16)
-    stacked_query = jnp.stack([queries * halves, queries * (1 - halves)], axis=2)
-    score_scale = half_width ** (-0.5)
-    own_scores = (
-        jnp.einsum("shcd,shd->shc", stacked_query, key_new, preferred_element_type=jnp.float32)
-        * score_scale
-    )
-    positions = lax.iota(jnp.int32, cache_len)
-    live_mask = (positions[None, :] < lengths[:, None])[:, None, None, :]
-    scores = (
-        jnp.einsum("shcd,slhd->shcl", stacked_query, key_cache, preferred_element_type=jnp.float32)
-        * score_scale
-    )
-    scores = jnp.where(live_mask, scores, -jnp.inf)
-    mix_weights, own_mixed = mixed_weights(scores, own_scores, mix_lambda)
-    heads_out = jnp.einsum(
-        "shl,slhd->shd", mix_weights, value_cache, preferred_element_type=jnp.float32
-    )
-    heads_out = heads_out + own_mixed.astype(jnp.float32)[..., None] * value_new.astype(jnp.float32)
-    normed_heads = (
-        heads_out
-        * lax.rsqrt(jnp.mean(heads_out * heads_out, axis=-1, keepdims=True) + epsilon)
-        * head_gain
-        * branch_scale
-    ).astype(jnp.bfloat16)
-    partial_value = jnp.dot(
-        normed_heads.reshape(seq_dev, columns),
-        w_out.reshape(columns, model_width),
-        preferred_element_type=jnp.float32,
-    )
-    partial_value = partial_value.astype(jnp.bfloat16)
     own_core = lax.axis_index("core")
     rows_y = lax.axis_size("y")
     width = model_width // (2 * rows_y)
@@ -115,17 +311,31 @@
     def swap_cores(source):
         return lax.ppermute(source, "core", [(0, 1), (1, 0)])
 
-    def pair_sum(source):
-        kept, sent = halves_of(source)
+    def add_swapped(kept, sent):
         arrived = swap_cores(sent)
         return (kept.astype(jnp.float32) + arrived.astype(jnp.float32)).astype(jnp.bfloat16)
 
-    pair = pair_sum(partial_value)
+    kept, sent = attend(
+        tokens,
+        lengths,
+        key_cache,
+        value_cache,
+        attn_gain,
+        w_query,
+        w_key,
+        w_value,
+        mix_lambda,
+        head_gain,
+        w_out,
+        rows_y,
+    )
+    pair = add_swapped(kept, sent)
     if rows_y == 2:
         other = lax.ppermute(pair, "y", [(0, 1), (1, 0)])
         attention = pair.astype(jnp.float32) + other.astype(jnp.float32)
     else:
         attention = jnp.sum(lax.all_gather(pair, "y").astype(jnp.float32), axis=0)
+    attention = attention.transpose(1, 0, 2)
     own_tokens, _ = halves_of(tokens)
     residual = (own_tokens.astype(jnp.float32) + attention).astype(jnp.bfloat16)
     half_width_all = rows_y * width
@@ -163,7 +373,7 @@
         jnp.bfloat16
     )
     pieces = jnp.dot(activated, w_down[0], preferred_element_type=jnp.float32).astype(jnp.bfloat16)
-    pieces = pair_sum(pieces).reshape(experts, capacity, rows_y, width)
+    pieces = add_swapped(*halves_of(pieces)).reshape(experts, capacity, rows_y, width)
     pieces = pieces.transpose(0, 2, 1, 3).reshape(experts * rows_y, capacity, width)
     returned = lax.all_to_all(pieces, ("ep", "y"), split_axis=0, concat_axis=0, tiled=True)
     returned = returned.reshape(experts, rows_y, capacity, width).astype(jnp.float32)

time: 65.6 us -> 60.6 us (0.924)
  matrix products: 19 us -> 3.56 us
  Pallas kernels: 0 us -> 13.1 us
  other arithmetic: 3.7 us -> 2.08 us
  local copies, waits for them, and re-layouts: 4.05 us -> 3.1 us
    dot_general x7 -> x0, matrix products: 14.5 us -> none  [the longest x1 5.84 us: per_device(): jnp.einsum('shcd,slhd->shcl', stacked_query, key_cache, preferred_element...]
    pallas_call x0 -> x1, Pallas kernels: none -> 13.1 us  [attend(): pl.pallas_call(attention_kernel, out_shape=(out, out), in_specs=[hbm] * 1...]
    dot_general x1, matrix products: 2.06 us -> 0.47 us  [per_device(): jnp.dot(normed_ffn, w_gate[0], preferred_element_type=jnp.float32)]
    reduce_sum x2 -> x1, other arithmetic: 1.34 us -> 0.23 us  [norm_rows(): jnp.mean(wide * wide, axis=-1, keepdims=True) + epsilon]
where the time goes in v2:
time: 60.6 us; the launch traced here: 60.3 us
  waiting for transfers between devices  15.6 us (26%)
  blocking collectives  14.3 us (24%)
  Pallas kernels  13.1 us (22%)
  starting transfers between devices  8.26 us (14%)
  matrix products  3.56 us (6%)
  local copies, waits for them, and re-layouts  3.1 us (5%)
  other arithmetic  2.08 us (3%)
    all_to_all x1, blocking collectives, per_device(): lax.all_to_all(outgoing, 'ep', split_axis=0, concat_axis=0, tiled=True)  14.3 us
    pallas_call x1, Pallas kernels, attend(): pl.pallas_call(attention_kernel, out_shape=(out, out), in_specs=[hbm] * 1...  13.1 us
    all_to_all x1, waiting for transfers between devices, per_device(): lax.all_to_all(pieces, ('ep', 'y'), split_axis=0, concat_axis=0, tiled=True)  10.1 us
    all_to_all x1, starting transfers between devices, per_device(): lax.all_to_all(pieces, ('ep', 'y'), split_axis=0, concat_axis=0, tiled=True)  4.5 us
    ppermute x3, waiting for transfers between devices, swap_cores(): return lax.ppermute(source, 'core', [(0, 1), (1, 0)])  3.67 us
    dot_general x1, matrix products, per_device(): jnp.dot(activated, w_down[0], preferred_element_type=jnp.float32)  3.09 us
    ppermute x1, starting transfers between devices, per_device(): other = lax.ppermute(pair, 'y', [(0, 1), (1, 0)])  2.91 us
    ppermute x1, waiting for transfers between devices, per_device(): other = lax.ppermute(pair, 'y', [(0, 1), (1, 0)])  1.82 us
  transfers between devices with their start and end apart: 5, of which 5 were waited for; matrix products, arithmetic and copies ran while one was open for 1% of the time, Pallas kernels for 0%

profile of v2, /device:TPU:0, one launch (start us, length us, event | category | flops | bytes accessed | tf_op | source)
XLA Modules:
  0.0 60.3 jit_solution(1788774800379904707)
XLA Ops:
  0.0 13.1 %attention.1 = (bf16[2,16,512]{2,1,0:T(8,128)(2,1)}, bf16[2,16,512]{2,1,0:T(8,128)(2,1)}) custom-call(s32[16]{0:T(128)} %lengths_hbm.1, f32[2]{0:T(128)} %lambda_hbm.1, bf16[16,2048]{1,0:T(8,128)(2,1)} %tokens_hbm.1, f32[1,2048]{1,0:T(1,128)} %bitcast.79, f32[1,128]{1,0:T(1,128)} %bitcast.80, bf16[4096,128]{1,0:T(8,128)(2,1)} %bitcast.70, ...), custom_call_target="tpu_custom_call" | custom-call | flops 4000000000 | bytes 16777216 | tf_op jit(solution)/shard_map/attention/pallas_call | solution.py:230
  13.1 0.6 collective-permute-start
  13.7 0.0 copy-done.1
  13.7 1.0 %collective-permute-done = bf16[2,16,512]{2,1,0:T(8,128)(2,1)S(1)} collective-permute-done((bf16[2,16,512]{2,1,0:T(8,128)(2,1)}, bf16[2,16,512]{2,1,0:T(8,128)(2,1)S(1)}, u32[]{:S(2)}, u32[]{:S(2)}) %collective-permute-start) | collective-permute-done | bytes 32800 | tf_op jit(solution)/shard_map/ppermute | solution.py:312
  14.7 0.8 %add_convert_fusion = bf16[2,16,512]{2,1,0:T(8,128)(2,1)S(1)} fusion(bf16[2,16,512]{2,1,0:T(8,128)(2,1)S(1)} %collective-permute-done, bf16[2,16,512]{2,1,0:T(8,128)(2,1)} %get-tuple-element.7), kind=kLoop, calls=%fused_computation.36 | loop fusion | flops 65536 | bytes 98304 | tf_op jit(solution)/shard_map/convert_element_type | solution.py:316
  15.5 2.9 %collective-permute-start.1 = (bf16[2,16,512]{2,1,0:T(8,128)(2,1)S(1)}, bf16[2,16,512]{2,1,0:T(8,128)(2,1)S(1)}, u32[]{:S(2)}, u32[]{:S(2)}) collective-permute-start(bf16[2,16,512]{2,1,0:T(8,128)(2,1)S(1)} %add_convert_fusion), channel_id=1, source_target_pairs={{0,2},{2,0},{1,3},{3,1},{4,6},{6,4},{5,7},{7,5},{8,10},{10,8},{9,1... | collective-permute-start | bytes 98312 | tf_op jit(solution)/shard_map/ppermute | solution.py:334
  18.4 0.1 constant_dynamic-slice_fusion.2
  18.5 1.8 %collective-permute-done.1 = bf16[2,16,512]{2,1,0:T(8,128)(2,1)S(1)} collective-permute-done((bf16[2,16,512]{2,1,0:T(8,128)(2,1)S(1)}, bf16[2,16,512]{2,1,0:T(8,128)(2,1)S(1)}, u32[]{:S(2)}, u32[]{:S(2)}) %collective-permute-start.1) | collective-permute-done | bytes 32800 | tf_op jit(solution)/shard_map/ppermute | solution.py:334
  20.4 14.3 %all_to_all.10 = bf16[8,16,1024]{2,1,0:T(8,128)(2,1)S(1)} all-to-all(bf16[8,16,1024]{2,1,0:T(8,128)(2,1)S(1)} %broadcast_in_dim.28), channel_id=1, replica_groups=mesh['ep'=8,'y'=2,'core'=2] {'ep'}, dimensions={0} | all-to-all | bytes 524288 | tf_op jit(solution)/shard_map/all_to_all | solution.py:357
  34.7 0.2 reshape.163
  34.9 0.1 collective-permute-start.2
  35.0 0.0 copy-start
  35.0 0.2 stack_reshape.4
  35.2 1.3 %collective-permute-done.2 = bf16[128,2,512]{2,1,0:T(2,128)(2,1)S(1)} collective-permute-done((bf16[128,2,512]{2,1,0:T(2,128)(2,1)S(1)}, bf16[128,2,512]{2,1,0:T(2,128)(2,1)S(1)}, u32[]{:S(2)}, u32[]{:S(2)}) %collective-permute-start.2) | collective-permute-done | bytes 262176 | tf_op jit(solution)/shard_map/ppermute | solution.py:312
  36.5 0.2 fusion.25
  36.8 0.2 fusion.27
  37.0 0.3 copy.59
  37.3 0.5 fusion.8
  37.7 3.1 %convolution_convert_fusion = bf16[128,2048]{1,0:T(8,128)(2,1)S(1)} fusion(bf16[1,512,2048]{2,1,0:T(8,128)(2,1)} %param.31, f32[128,512]{1,0:T(8,128)S(1)} %fusion.8, bf16[128,2048]{0,1:T(8,128)(2,1)S(1)} %bitcast.67, bf16[1,2048,512]{2,1,0:T(8,128)(2,1)} %param.30), kind=kOutput, calls=%fused_computation | convolution fusion | flops 537722880 | bytes 5505024 | tf_op jit(solution)/shard_map/dot_general | solution.py:375
  40.8 0.4 reshape.164
  41.2 0.0 copy-start.3
  41.2 0.0 copy-start.4
  41.2 1.1 %constant_dynamic-slice_fusion.1 = (bf16[128,2,1,512]{3,2,1,0:T(2,128)(2,1)S(1)}, bf16[128,2,1,512]{3,2,1,0:T(2,128)(2,1)S(1)}) fusion(bf16[128,2,2,512]{3,2,1,0:T(2,128)(2,1)S(1)} %reshape.164, s32[]{:T(128)S(6)} %select_n.38, s32[]{:T(128)S(6)} %select_n.43), kind=kLoop, calls=%fused_computation.43 | loop fusion | bytes 1048584 | tf_op jit(solution)/shard_map/jit(dynamic_index_in_dim)/dynamic_slice | solution.py:307
  42.3 0.1 copy.75
  42.4 0.2 collective-permute-start.3
  42.6 1.4 %collective-permute-done.3 = bf16[128,2,512]{2,0,1:T(8,128)(2,1)S(1)} collective-permute-done((bf16[128,2,512]{2,0,1:T(8,128)(2,1)S(1)}, bf16[128,2,512]{2,0,1:T(8,128)(2,1)S(1)}, u32[]{:S(2)}, u32[]{:S(2)}) %collective-permute-start.3) | collective-permute-done | bytes 262176 | tf_op jit(solution)/shard_map/ppermute | solution.py:312
  44.0 0.1 fusion.28
  44.1 0.7 %copy.62 = bf16[8,16,2,512]{3,1,2,0:T(8,128)(2,1)} copy(bf16[8,16,2,512]{3,1,0,2:T(8,128)(2,1)S(1)} %bitcast.74) | data formatting | bytes 524288 | tf_op jit(solution)/shard_map/reshape | solution.py:376
  44.8 4.5 %all-to-all-start.1 = ((bf16[16,16,512]{2,1,0:T(8,128)(2,1)}), bf16[16,16,512]{2,1,0:T(8,128)(2,1)S(1)}, u32[]{:S(2)}, u32[]{:S(2)}) async-start(bf16[16,16,512]{2,1,0:T(8,128)(2,1)} %bitcast.21), calls=%async_computation.1 | async-start | bytes 524288 | tf_op jit(solution)/shard_map/all_to_all | solution.py:378
  49.4 10.1 %all-to-all-done.1 = bf16[16,16,512]{2,1,0:T(8,128)(2,1)S(1)} async-done(((bf16[16,16,512]{2,1,0:T(8,128)(2,1)}), bf16[16,16,512]{2,1,0:T(8,128)(2,1)S(1)}, u32[]{:S(2)}, u32[]{:S(2)}) %all-to-all-start.1) | async-done | bytes 262176 | tf_op jit(solution)/shard_map/all_to_all | solution.py:378
  59.6 0.1 multiply_reduce_fusion
  59.7 0.6 %fusion.39 = bf16[16,512]{1,0:T(8,128)(2,1)} fusion(f32[16,512]{1,0:T(8,128)S(1)} %multiply_reduce_fusion, bf16[16,2,512]{2,0,1:T(8,128)(2,1)S(1)} %fusion.38, s32[]{:T(128)S(6)} %select_n.39), kind=kLoop, calls=%fused_computation.39 | loop fusion | flops 24576 | bytes 65540 | tf_op jit(solution)/shard_map/convert_element_type | solution.py:391
  (16 shorter events, 0.2 us)
Async XLA Ops:
  0.0 13.7 %copy-start.1 = (bf16[16,2048]{1,0:T(8,128)(2,1)S(1)}, bf16[16,2048]{1,0:T(8,128)(2,1)}, u32[]{:S(2)}) copy-start(bf16[16,2048]{1,0:T(8,128)(2,1)} %tokens_hbm.1) | copy-start | bytes 196612
  0.0 35.0 %copy-start.2 = (f32[2048]{0:T(1024)S(1)}, f32[2048]{0:T(1024)}, u32[]{:S(2)}) copy-start(f32[2048]{0:T(1024)} %param.28) | copy-start | bytes 24580
  13.1 1.6 %collective-permute-start = (bf16[2,16,512]{2,1,0:T(8,128)(2,1)}, bf16[2,16,512]{2,1,0:T(8,128)(2,1)S(1)}, u32[]{:S(2)}, u32[]{:S(2)}) collective-permute-start(bf16[2,16,512]{2,1,0:T(8,128)(2,1)} %get-tuple-element.8), channel_id=1, source_target_pairs={{0,1},{1,0},{2,3},{3,2},{4,5},{5,4},{6,7},{7,6},{8,9},{9,8},{10,11... | collective-permute-start | bytes 98312 | tf_op jit(solution)/shard_map/ppermute | solution.py:312
  15.5 4.8 %collective-permute-start.1 = (bf16[2,16,512]{2,1,0:T(8,128)(2,1)S(1)}, bf16[2,16,512]{2,1,0:T(8,128)(2,1)S(1)}, u32[]{:S(2)}, u32[]{:S(2)}) collective-permute-start(bf16[2,16,512]{2,1,0:T(8,128)(2,1)S(1)} %add_convert_fusion), channel_id=1, source_target_pairs={{0,2},{2,0},{1,3},{3,1},{4,6},{6,4},{5,7},{7,5},{8,10},{10,8},{9,1... | collective-permute-start | bytes 98312 | tf_op jit(solution)/shard_map/ppermute | solution.py:334
  34.9 1.6 %collective-permute-start.2 = (bf16[128,2,512]{2,1,0:T(2,128)(2,1)S(1)}, bf16[128,2,512]{2,1,0:T(2,128)(2,1)S(1)}, u32[]{:S(2)}, u32[]{:S(2)}) collective-permute-start(bf16[128,2,512]{2,1,0:T(2,128)(2,1)S(1)} %reshape.163), channel_id=1, source_target_pairs={{0,1},{1,0},{2,3},{3,2},{4,5},{5,4},{6,7},{7,6},{8,9},{9,8},{10,11... | collective-permute-start | bytes 786440 | tf_op jit(solution)/shard_map/ppermute | solution.py:312
  35.0 2.2 %copy-start = (bf16[1,2048,512]{2,1,0:T(8,128)(2,1)S(1)}, bf16[1,2048,512]{2,1,0:T(8,128)(2,1)}, u32[]{:S(2)}) copy-start(bf16[1,2048,512]{2,1,0:T(8,128)(2,1)} %param.29) | copy-start | bytes 6291460
  41.2 8.1 %copy-start.3 = (f32[16,4]{0,1:T(4,128)S(1)}, f32[16,4]{0,1:T(4,128)}, u32[]{:S(2)}) copy-start(f32[16,4]{0,1:T(4,128)} %param.33) | copy-start | bytes 772
  41.2 8.1 %copy-start.4 = (s32[16,4]{0,1:T(4,128)S(1)}, s32[16,4]{0,1:T(4,128)}, u32[]{:S(2)}) copy-start(s32[16,4]{0,1:T(4,128)} %param.32) | copy-start | bytes 772
  42.4 1.6 %collective-permute-start.3 = (bf16[128,2,512]{2,0,1:T(8,128)(2,1)S(1)}, bf16[128,2,512]{2,0,1:T(8,128)(2,1)S(1)}, u32[]{:S(2)}, u32[]{:S(2)}) collective-permute-start(bf16[128,2,512]{2,0,1:T(8,128)(2,1)S(1)} %bitcast.75), channel_id=1, source_target_pairs={{0,1},{1,0},{2,3},{3,2},{4,5},{5,4},{6,7},{7,6},{8,9},{9,8},{10,11... | collective-permute-start | bytes 786440 | tf_op jit(solution)/shard_map/ppermute | solution.py:312
  44.8 14.7 %all-to-all-start.1 = ((bf16[16,16,512]{2,1,0:T(8,128)(2,1)}), bf16[16,16,512]{2,1,0:T(8,128)(2,1)S(1)}, u32[]{:S(2)}, u32[]{:S(2)}) async-start(bf16[16,16,512]{2,1,0:T(8,128)(2,1)} %bitcast.21), calls=%async_computation.1 | async-start | bytes 524288 | tf_op jit(solution)/shard_map/all_to_all | solution.py:378

commit v3 on v2

--- a/solution.py
+++ b/solution.py
@@ -84,10 +84,12 @@
             )
         )
     ]
-    for copy in large:
-        copy.start()
+    for i in (0, 1, 2, 3):
+        large[i].start()
     for copy in small:
         copy.wait()
+    large[4].start()
+    large[5].start()
     normed = norm_rows(tokens_ref[...], gain_ref[...]).astype(bf16)
     spread = (
         lax.broadcasted_iota(jnp.int32, (lanes, heads * lanes), 1) // heads
@@ -275,6 +277,64 @@
 attention_flops = 4 * 10**9
 
 
+def expert_kernel(own_ref, other_ref, gain_ref, gate_ref, up_ref, down_ref, kept_ref, sent_ref):
+    rows_y, _, width = kept_ref.shape
+    model_width = gain_ref.shape[1]
+    f32, bf16 = jnp.float32, jnp.bfloat16
+    core = lax.axis_index("core")
+    sides = ((own_ref, core), (other_ref, 1 - core))
+
+    def columns(y, which):
+        return pl.ds(pl.multiple_of((2 * y + which) * width, width), width)
+
+    total = 0.0
+    for source, _ in sides:
+        wide = source[...].astype(f32)
+        total = total + jnp.sum(wide * wide, axis=-1, keepdims=True)
+    scale = lax.rsqrt(total / model_width + epsilon)
+    gate_value, up_value = 0.0, 0.0
+    for source, which in sides:
+        for y in range(rows_y):
+            at = columns(y, which)
+            wide = source[:, y * width : (y + 1) * width].astype(f32)
+            normed = (wide * scale * gain_ref[:, at]).astype(bf16)
+            gate_value = gate_value + jnp.dot(normed, gate_ref[at, :], preferred_element_type=f32)
+            up_value = up_value + jnp.dot(normed, up_ref[at, :], preferred_element_type=f32)
+    gate_value = jnp.minimum(gate_value, clamp_limit)
+    up_value = jnp.clip(up_value, -clamp_limit, clamp_limit)
+    activated = ((up_value + 1.0) * gate_value * jax.nn.sigmoid(sigmoid_slope * gate_value)).astype(
+        bf16
+    )
+    for target, which in ((sent_ref, 1 - core), (kept_ref, core)):
+        for y in range(rows_y):
+            target[y] = jnp.dot(
+                activated, down_ref[:, columns(y, which)], preferred_element_type=f32
+            ).astype(bf16)
+
+
+def apply_expert(own, other, ffn_gain, w_gate, w_up, w_down, rows_y):
+    rows, half = own.shape
+    model_width, hidden = w_gate.shape
+    out = jax.ShapeDtypeStruct((rows_y, rows, half // rows_y), jnp.bfloat16)
+    vmem = pl.BlockSpec(memory_space=pltpu.VMEM)
+    return pl.pallas_call(
+        expert_kernel,
+        out_shape=(out, out),
+        in_specs=[vmem] * 6,
+        out_specs=(vmem, vmem),
+        compiler_params=pltpu.CompilerParams(vmem_limit_bytes=expert_vmem),
+        cost_estimate=pl.CostEstimate(
+            flops=6 * rows * model_width * hidden,
+            bytes_accessed=6 * model_width * hidden,
+            transcendentals=rows * hidden,
+        ),
+        name="expert",
+    )(own, other, ffn_gain.reshape(1, model_width), w_gate, w_up, w_down)
+
+
+expert_vmem = 24 * 1024 * 1024
+
+
 def per_device(
     tokens,
     lengths,
@@ -355,29 +415,14 @@
     else:
         outgoing = jnp.broadcast_to(flat_residual[None], (experts, seq_dev, half_width_all))
     arrived = lax.all_to_all(outgoing, "ep", split_axis=0, concat_axis=0, tiled=True)
-    own_half = arrived.reshape(experts * capacity, rows_y, width)
-    other_half = swap_cores(own_half)
-    flat_rows = jnp.where(
-        own_core == 0,
-        jnp.stack([own_half, other_half], axis=2),
-        jnp.stack([other_half, own_half], axis=2),
-    ).reshape(experts * capacity, model_width)
-    normed_ffn = norm_rows(flat_rows, ffn_gain).astype(jnp.bfloat16)
-    gate_value = jnp.minimum(
-        jnp.dot(normed_ffn, w_gate[0], preferred_element_type=jnp.float32), clamp_limit
-    )
-    up_value = jnp.clip(
-        jnp.dot(normed_ffn, w_up[0], preferred_element_type=jnp.float32), -clamp_limit, clamp_limit
-    )
-    activated = ((up_value + 1.0) * gate_value * jax.nn.sigmoid(sigmoid_slope * gate_value)).astype(
-        jnp.bfloat16
-    )
-    pieces = jnp.dot(activated, w_down[0], preferred_element_type=jnp.float32).astype(jnp.bfloat16)
-    pieces = add_swapped(*halves_of(pieces)).reshape(experts, capacity, rows_y, width)
-    pieces = pieces.transpose(0, 2, 1, 3).reshape(experts * rows_y, capacity, width)
-    returned = lax.all_to_all(pieces, ("ep", "y"), split_axis=0, concat_axis=0, tiled=True)
-    returned = returned.reshape(experts, rows_y, capacity, width).astype(jnp.float32)
-    expert_out = jnp.sum(returned, axis=1).astype(jnp.bfloat16).astype(jnp.float32)
+    own_half = arrived.reshape(experts * capacity, half_width_all)
+    kept, sent = apply_expert(
+        own_half, swap_cores(own_half), ffn_gain, w_gate[0], w_up[0], w_down[0], rows_y
+    )
+    pieces = add_swapped(kept, sent).reshape(rows_y * experts, capacity, width)
+    returned = lax.all_to_all(pieces, ("y", "ep"), split_axis=0, concat_axis=0, tiled=True)
+    returned = returned.reshape(rows_y, experts, capacity, width).astype(jnp.float32)
+    expert_out = jnp.sum(returned, axis=0).astype(jnp.bfloat16).astype(jnp.float32)
     if capacity < seq_dev:
         combine = jnp.sum(route_weights[..., None] * chosen, axis=1)
         expert_sum = jnp.dot(

time: 60.6 us -> 56.9 us (0.939)
  matrix products: 3.56 us -> 0 us
  Pallas kernels: 13.1 us -> 10.7 us
  local copies, waits for them, and re-layouts: 3.1 us -> 4.92 us
    unnamed x11 -> x14, local copies, waits for them, and re-layouts: 0.11 us -> 4.79 us
    pallas_call x1, Pallas kernels: 13.1 us -> 9.47 us  [attend(): pl.pallas_call(attention_kernel, out_shape=(out, out), in_specs=[hbm] * 1...]
    dot_general x2 -> x0, matrix products: 3.56 us -> none  [the longest x1 3.09 us: per_device(): jnp.dot(activated, w_down[0], preferred_element_type=jnp.float32)]
    pallas_call x0 -> x1, Pallas kernels: none -> 1.25 us  [apply_expert(): pl.pallas_call(expert_kernel, out_shape=(out, out), in_specs=[vmem] * 6,...]
    dynamic_slice x2 -> x1, local copies, waits for them, and re-layouts: 1.16 us -> 0.07 us  [halves_of(): kept = lax.dynamic_index_in_dim(blocks, own_core, 2, keepdims=False)]
    reshape x2 -> x0, local copies, waits for them, and re-layouts: 0.88 us -> none  [the longest x1 0.71 us: per_device(): add_swapped(*halves_of(pieces)).reshape(experts, capacity, rows_y, width)]
    convert_element_type x2, other arithmetic: 0.88 us -> 1.53 us  [add_swapped(): (kept.astype(jnp.float32) + arrived.astype(jnp.float32)).astype(jnp.bfloa...]
  transfers between devices with their start and end apart: 5 -> 5, of which waited for: 5 -> 5; matrix products, arithmetic and copies ran while one was open for 1% -> 0% of each run, Pallas kernels for 0% -> 0%
where the time goes in v3:
time: 56.9 us; the launch traced here: 56.5 us
  waiting for transfers between devices  15.9 us (28%)
  blocking collectives  14.3 us (25%)
  Pallas kernels  10.7 us (19%)
  starting transfers between devices  8.19 us (14%)
  local copies, waits for them, and re-layouts  4.92 us (9%)
  other arithmetic  2.31 us (4%)
    all_to_all x1, blocking collectives, per_device(): lax.all_to_all(outgoing, 'ep', split_axis=0, concat_axis=0, tiled=True)  14.3 us
    all_to_all x1, waiting for transfers between devices, per_device(): lax.all_to_all(pieces, ('y', 'ep'), split_axis=0, concat_axis=0, tiled=True)  10.1 us
    pallas_call x1, Pallas kernels, attend(): pl.pallas_call(attention_kernel, out_shape=(out, out), in_specs=[hbm] * 1...  9.47 us
    unnamed x14, local copies, waits for them, and re-layouts  4.79 us
    all_to_all x1, starting transfers between devices, per_device(): lax.all_to_all(pieces, ('y', 'ep'), split_axis=0, concat_axis=0, tiled=True)  4.5 us
    ppermute x3, waiting for transfers between devices, swap_cores(): return lax.ppermute(source, 'core', [(0, 1), (1, 0)])  3.95 us
    ppermute x1, starting transfers between devices, per_device(): other = lax.ppermute(pair, 'y', [(0, 1), (1, 0)])  2.92 us
    ppermute x1, waiting for transfers between devices, per_device(): other = lax.ppermute(pair, 'y', [(0, 1), (1, 0)])  1.82 us
  transfers between devices with their start and end apart: 5, of which 5 were waited for; matrix products, arithmetic and copies ran while one was open for 0% of the time, Pallas kernels for 0%

profile of v3, /device:TPU:0, one launch (start us, length us, event | category | flops | bytes accessed | tf_op | source)
XLA Modules:
  0.0 56.5 jit_solution(18380332958516651964)
XLA Ops:
  0.0 0.0 copy-start.4
  0.0 0.0 copy-start.3
  0.0 9.5 %attention.1 = (bf16[2,16,512]{2,1,0:T(8,128)(2,1)}, bf16[2,16,512]{2,1,0:T(8,128)(2,1)}) custom-call(s32[16]{0:T(128)} %lengths_hbm.1, f32[2]{0:T(128)} %lambda_hbm.1, bf16[16,2048]{1,0:T(8,128)(2,1)} %tokens_hbm.1, f32[1,2048]{1,0:T(1,128)} %bitcast.44, f32[1,128]{1,0:T(1,128)} %bitcast.45, bf16[4096,128]{1,0:T(8,128)(2,1)} %bitcast.36, ...), custom_call_target="tpu_custom_call" | custom-call | flops 4000000000 | bytes 16777216 | tf_op jit(solution)/shard_map/attention/pallas_call | solution.py:232
  9.5 0.6 collective-permute-start
  10.0 0.0 copy-done.4
  10.1 1.0 %collective-permute-done = bf16[2,16,512]{2,1,0:T(8,128)(2,1)S(1)} collective-permute-done((bf16[2,16,512]{2,1,0:T(8,128)(2,1)}, bf16[2,16,512]{2,1,0:T(8,128)(2,1)S(1)}, u32[]{:S(2)}, u32[]{:S(2)}) %collective-permute-start) | collective-permute-done | bytes 32800 | tf_op jit(solution)/shard_map/ppermute | solution.py:372
  11.1 0.8 %add_convert_fusion.1 = bf16[2,16,512]{2,1,0:T(8,128)(2,1)S(1)} fusion(bf16[2,16,512]{2,1,0:T(8,128)(2,1)S(1)} %collective-permute-done, bf16[2,16,512]{2,1,0:T(8,128)(2,1)} %get-tuple-element.9), kind=kLoop, calls=%fused_computation.4 | loop fusion | flops 65536 | bytes 98304 | tf_op jit(solution)/shard_map/convert_element_type | solution.py:376
  11.9 2.9 %collective-permute-start.1 = (bf16[2,16,512]{2,1,0:T(8,128)(2,1)S(1)}, bf16[2,16,512]{2,1,0:T(8,128)(2,1)S(1)}, u32[]{:S(2)}, u32[]{:S(2)}) collective-permute-start(bf16[2,16,512]{2,1,0:T(8,128)(2,1)S(1)} %add_convert_fusion.1), channel_id=1, source_target_pairs={{0,2},{2,0},{1,3},{3,1},{4,6},{6,4},{5,7},{7,5},{8,10},{10,8},{9,1... | collective-permute-start | bytes 98312 | tf_op jit(solution)/shard_map/ppermute | solution.py:394
  14.8 0.1 constant_dynamic-slice_fusion
  14.9 1.8 %collective-permute-done.1 = bf16[2,16,512]{2,1,0:T(8,128)(2,1)S(1)} collective-permute-done((bf16[2,16,512]{2,1,0:T(8,128)(2,1)S(1)}, bf16[2,16,512]{2,1,0:T(8,128)(2,1)S(1)}, u32[]{:S(2)}, u32[]{:S(2)}) %collective-permute-start.1) | collective-permute-done | bytes 32800 | tf_op jit(solution)/shard_map/ppermute | solution.py:394
  16.8 14.3 %all_to_all.10 = bf16[8,16,1024]{2,1,0:T(8,128)(2,1)S(1)} all-to-all(bf16[8,16,1024]{2,1,0:T(8,128)(2,1)S(1)} %broadcast_in_dim.26), channel_id=1, replica_groups=mesh['ep'=8,'y'=2,'core'=2] {'ep'}, dimensions={0} | all-to-all | bytes 524288 | tf_op jit(solution)/shard_map/all_to_all | solution.py:417
  31.1 0.0 collective-permute-start.2
  31.1 1.5 %collective-permute-done.2.other_ref = bf16[128,1024]{1,0:T(8,128)(2,1)S(1)} collective-permute-done((bf16[128,1024]{1,0:T(8,128)(2,1)S(1)}, bf16[128,1024]{1,0:T(8,128)(2,1)S(1)}, u32[]{:S(2)}, u32[]{:S(2)}) %collective-permute-start.2) | collective-permute-done | bytes 262176 | tf_op jit(solution)/shard_map/ppermute | solution.py:372
  32.6 0.0 copy-done.3
  32.6 0.0 copy-start
  32.6 1.6 %copy-done = bf16[1,2048,512]{2,1,0:T(8,128)(2,1)S(1)} copy-done((bf16[1,2048,512]{2,1,0:T(8,128)(2,1)S(1)}, bf16[1,2048,512]{2,1,0:T(8,128)(2,1)}, u32[]{:S(2)}) %copy-start) | copy-done | bytes 2097176
  34.2 0.0 copy-start.1
  34.2 1.6 %copy-done.1 = bf16[1,2048,512]{2,1,0:T(8,128)(2,1)S(1)} copy-done((bf16[1,2048,512]{2,1,0:T(8,128)(2,1)S(1)}, bf16[1,2048,512]{2,1,0:T(8,128)(2,1)}, u32[]{:S(2)}) %copy-start.1) | copy-done | bytes 2097176
  35.8 0.0 copy-start.2
  35.8 1.6 %copy-done.2 = bf16[1,512,2048]{2,1,0:T(8,128)(2,1)S(1)} copy-done((bf16[1,512,2048]{2,1,0:T(8,128)(2,1)S(1)}, bf16[1,512,2048]{2,1,0:T(8,128)(2,1)}, u32[]{:S(2)}) %copy-start.2) | copy-done | bytes 2097176
  37.4 0.0 copy-start.5
  37.4 0.0 copy-start.6
  37.4 1.2 %expert.1 = (bf16[2,128,512]{2,1,0:T(8,128)(2,1)S(1)}, bf16[2,128,512]{2,1,0:T(8,128)(2,1)S(1)}) custom-call(bf16[128,1024]{1,0:T(8,128)(2,1)S(1)} %bitcast.32, bf16[128,1024]{1,0:T(8,128)(2,1)S(1)} %collective-permute-done.2.other_ref, f32[1,2048]{1,0:T(1,128)S(1)} %bitcast.33, bf16[2048,512]{1,0:T(8,128)(2,1)S(1)} %bitcast.28, ...), custom_call_target="tpu_custom_call" | custom-call | flops 805306368 | bytes 6291456 | tf_op jit(solution)/shard_map/expert/pallas_call | solution.py:320
  38.7 0.2 collective-permute-start.3
  38.9 1.4 %collective-permute-done.3 = bf16[2,128,512]{2,1,0:T(8,128)(2,1)S(1)} collective-permute-done((bf16[2,128,512]{2,1,0:T(8,128)(2,1)S(1)}, bf16[2,128,512]{2,1,0:T(8,128)(2,1)S(1)}, u32[]{:S(2)}, u32[]{:S(2)}) %collective-permute-start.3) | collective-permute-done | bytes 262176 | tf_op jit(solution)/shard_map/ppermute | solution.py:372
  40.3 0.8 %add_convert_fusion = bf16[2,128,512]{2,1,0:T(8,128)(2,1)} fusion(bf16[2,128,512]{2,1,0:T(8,128)(2,1)S(1)} %collective-permute-done.3, bf16[2,128,512]{2,1,0:T(8,128)(2,1)S(1)} %get-tuple-element.11), kind=kLoop, calls=%fused_computation | loop fusion | flops 524288 | bytes 786432 | tf_op jit(solution)/shard_map/convert_element_type | solution.py:376
  41.0 4.5 %all-to-all-start.1 = ((bf16[16,16,512]{2,1,0:T(8,128)(2,1)}), bf16[16,16,512]{2,1,0:T(8,128)(2,1)S(1)}, u32[]{:S(2)}, u32[]{:S(2)}) async-start(bf16[16,16,512]{2,1,0:T(8,128)(2,1)} %bitcast.17), calls=%async_computation.1 | async-start | bytes 524288 | tf_op jit(solution)/shard_map/all_to_all | solution.py:423
  45.6 0.0 copy-done.5
  45.6 0.0 copy-done.6
  45.6 10.1 %all-to-all-done.1 = bf16[16,16,512]{2,1,0:T(8,128)(2,1)S(1)} async-done(((bf16[16,16,512]{2,1,0:T(8,128)(2,1)}), bf16[16,16,512]{2,1,0:T(8,128)(2,1)S(1)}, u32[]{:S(2)}, u32[]{:S(2)}) %all-to-all-start.1) | async-done | bytes 262176 | tf_op jit(solution)/shard_map/all_to_all | solution.py:423
  55.8 0.1 multiply_reduce_fusion
  55.9 0.6 %fusion.1 = bf16[16,512]{1,0:T(8,128)(2,1)} fusion(f32[16,512]{1,0:T(8,128)S(1)} %multiply_reduce_fusion, bf16[16,2,512]{2,0,1:T(8,128)(2,1)S(1)} %fusion, s32[]{:T(128)S(6)} %select_n.13), kind=kLoop, calls=%fused_computation.7 | loop fusion | flops 24576 | bytes 65540 | tf_op jit(solution)/shard_map/convert_element_type | solution.py:436
  (6 shorter events, 0.1 us)
Async XLA Ops:
  0.0 10.0 %copy-start.4 = (bf16[16,2048]{1,0:T(8,128)(2,1)S(1)}, bf16[16,2048]{1,0:T(8,128)(2,1)}, u32[]{:S(2)}) copy-start(bf16[16,2048]{1,0:T(8,128)(2,1)} %tokens_hbm.1) | copy-start | bytes 196612
  0.0 32.6 %copy-start.3 = (f32[2048]{0:T(1024)S(1)}, f32[2048]{0:T(1024)}, u32[]{:S(2)}) copy-start(f32[2048]{0:T(1024)} %param.28) | copy-start | bytes 24580
  9.5 1.6 %collective-permute-start = (bf16[2,16,512]{2,1,0:T(8,128)(2,1)}, bf16[2,16,512]{2,1,0:T(8,128)(2,1)S(1)}, u32[]{:S(2)}, u32[]{:S(2)}) collective-permute-start(bf16[2,16,512]{2,1,0:T(8,128)(2,1)} %get-tuple-element.10), channel_id=1, source_target_pairs={{0,1},{1,0},{2,3},{3,2},{4,5},{5,4},{6,7},{7,6},{8,9},{9,8},{10,11... | collective-permute-start | bytes 98312 | tf_op jit(solution)/shard_map/ppermute | solution.py:372
  11.9 4.8 %collective-permute-start.1 = (bf16[2,16,512]{2,1,0:T(8,128)(2,1)S(1)}, bf16[2,16,512]{2,1,0:T(8,128)(2,1)S(1)}, u32[]{:S(2)}, u32[]{:S(2)}) collective-permute-start(bf16[2,16,512]{2,1,0:T(8,128)(2,1)S(1)} %add_convert_fusion.1), channel_id=1, source_target_pairs={{0,2},{2,0},{1,3},{3,1},{4,6},{6,4},{5,7},{7,5},{8,10},{10,8},{9,1... | collective-permute-start | bytes 98312 | tf_op jit(solution)/shard_map/ppermute | solution.py:394
  31.1 1.5 %collective-permute-start.2 = (bf16[128,1024]{1,0:T(8,128)(2,1)S(1)}, bf16[128,1024]{1,0:T(8,128)(2,1)S(1)}, u32[]{:S(2)}, u32[]{:S(2)}) collective-permute-start(bf16[128,1024]{1,0:T(8,128)(2,1)S(1)} %bitcast.31), channel_id=1, source_target_pairs={{0,1},{1,0},{2,3},{3,2},{4,5},{5,4},{6,7},{7,6},{8,9},{9,8},{10,11... | collective-permute-start | bytes 786440 | tf_op jit(solution)/shard_map/ppermute | solution.py:372
  32.6 1.6 %copy-start = (bf16[1,2048,512]{2,1,0:T(8,128)(2,1)S(1)}, bf16[1,2048,512]{2,1,0:T(8,128)(2,1)}, u32[]{:S(2)}) copy-start(bf16[1,2048,512]{2,1,0:T(8,128)(2,1)} %param.29) | copy-start | bytes 6291460
  34.2 1.6 %copy-start.1 = (bf16[1,2048,512]{2,1,0:T(8,128)(2,1)S(1)}, bf16[1,2048,512]{2,1,0:T(8,128)(2,1)}, u32[]{:S(2)}) copy-start(bf16[1,2048,512]{2,1,0:T(8,128)(2,1)} %param.30) | copy-start | bytes 6291460
  35.8 1.6 %copy-start.2 = (bf16[1,512,2048]{2,1,0:T(8,128)(2,1)S(1)}, bf16[1,512,2048]{2,1,0:T(8,128)(2,1)}, u32[]{:S(2)}) copy-start(bf16[1,512,2048]{2,1,0:T(8,128)(2,1)} %param.31) | copy-start | bytes 6291460
  37.4 8.1 %copy-start.5 = (f32[16,4]{0,1:T(4,128)S(1)}, f32[16,4]{0,1:T(4,128)}, u32[]{:S(2)}) copy-start(f32[16,4]{0,1:T(4,128)} %param.33) | copy-start | bytes 772
  37.4 8.1 %copy-start.6 = (s32[16,4]{0,1:T(4,128)S(1)}, s32[16,4]{0,1:T(4,128)}, u32[]{:S(2)}) copy-start(s32[16,4]{0,1:T(4,128)} %param.32) | copy-start | bytes 772
  38.7 1.6 %collective-permute-start.3 = (bf16[2,128,512]{2,1,0:T(8,128)(2,1)S(1)}, bf16[2,128,512]{2,1,0:T(8,128)(2,1)S(1)}, u32[]{:S(2)}, u32[]{:S(2)}) collective-permute-start(bf16[2,128,512]{2,1,0:T(8,128)(2,1)S(1)} %get-tuple-element.12), channel_id=1, source_target_pairs={{0,1},{1,0},{2,3},{3,2},{4,5},{5,4},{6,7},{7,6},{8,9},{9,8},{10,11... | collective-permute-start | bytes 786440 | tf_op jit(solution)/shard_map/ppermute | solution.py:372
  41.0 14.7 %all-to-all-start.1 = ((bf16[16,16,512]{2,1,0:T(8,128)(2,1)}), bf16[16,16,512]{2,1,0:T(8,128)(2,1)S(1)}, u32[]{:S(2)}, u32[]{:S(2)}) async-start(bf16[16,16,512]{2,1,0:T(8,128)(2,1)} %bitcast.17), calls=%async_computation.1 | async-start | bytes 524288 | tf_op jit(solution)/shard_map/all_to_all | solution.py:423

commit v4 on v3

--- a/solution.py
+++ b/solution.py
@@ -277,7 +277,28 @@
 attention_flops = 4 * 10**9
 
 
-def expert_kernel(own_ref, other_ref, gain_ref, gate_ref, up_ref, down_ref, kept_ref, sent_ref):
+def expert_kernel(
+    own_ref,
+    other_ref,
+    gain_ref,
+    gate_hbm,
+    up_hbm,
+    down_hbm,
+    kept_ref,
+    sent_ref,
+    gate_ref,
+    up_ref,
+    down_ref,
+    weight_sem,
+):
+    copies = [
+        pltpu.make_async_copy(source, target, weight_sem.at[i])
+        for i, (source, target) in enumerate(
+            ((gate_hbm, gate_ref), (up_hbm, up_ref), (down_hbm, down_ref))
+        )
+    ]
+    for copy in copies:
+        copy.start()
     rows_y, _, width = kept_ref.shape
     model_width = gain_ref.shape[1]
     f32, bf16 = jnp.float32, jnp.bfloat16
@@ -292,19 +313,26 @@
         wide = source[...].astype(f32)
         total = total + jnp.sum(wide * wide, axis=-1, keepdims=True)
     scale = lax.rsqrt(total / model_width + epsilon)
-    gate_value, up_value = 0.0, 0.0
+    normed = []
     for source, which in sides:
         for y in range(rows_y):
             at = columns(y, which)
             wide = source[:, y * width : (y + 1) * width].astype(f32)
-            normed = (wide * scale * gain_ref[:, at]).astype(bf16)
-            gate_value = gate_value + jnp.dot(normed, gate_ref[at, :], preferred_element_type=f32)
-            up_value = up_value + jnp.dot(normed, up_ref[at, :], preferred_element_type=f32)
+            normed.append(((wide * scale * gain_ref[:, at]).astype(bf16), at))
+    products = []
+    for copy, weight in zip(copies, (gate_ref, up_ref)):
+        copy.wait()
+        product = 0.0
+        for part, at in normed:
+            product = product + jnp.dot(part, weight[at, :], preferred_element_type=f32)
+        products.append(product)
+    gate_value, up_value = products
     gate_value = jnp.minimum(gate_value, clamp_limit)
     up_value = jnp.clip(up_value, -clamp_limit, clamp_limit)
     activated = ((up_value + 1.0) * gate_value * jax.nn.sigmoid(sigmoid_slope * gate_value)).astype(
         bf16
     )
+    copies[2].wait()
     for target, which in ((sent_ref, 1 - core), (kept_ref, core)):
         for y in range(rows_y):
             target[y] = jnp.dot(
@@ -320,8 +348,14 @@
     return pl.pallas_call(
         expert_kernel,
         out_shape=(out, out),
-        in_specs=[vmem] * 6,
+        in_specs=[vmem] * 3 + [pl.BlockSpec(memory_space=pltpu.HBM)] * 3,
         out_specs=(vmem, vmem),
+        scratch_shapes=[
+            pltpu.VMEM((model_width, hidden), jnp.bfloat16),
+            pltpu.VMEM((model_width, hidden), jnp.bfloat16),
+            pltpu.VMEM((hidden, model_width), jnp.bfloat16),
+            pltpu.SemaphoreType.DMA((3,)),
+        ],
         compiler_params=pltpu.CompilerParams(vmem_limit_bytes=expert_vmem),
         cost_estimate=pl.CostEstimate(
             flops=6 * rows * model_width * hidden,
@@ -332,7 +366,7 @@
     )(own, other, ffn_gain.reshape(1, model_width), w_gate, w_up, w_down)
 
 
-expert_vmem = 24 * 1024 * 1024
+expert_vmem = 53 * 1024 * 1024
 
 
 def per_device(

time: 56.9 us -> 55.8 us (0.981)
  local copies, waits for them, and re-layouts: 4.92 us -> 0.83 us
  Pallas kernels: 10.7 us -> 13.8 us
    unnamed x14 -> x10, local copies, waits for them, and re-layouts: 4.79 us -> 0.71 us
    pallas_call x1, Pallas kernels: 1.25 us -> 4.32 us  [apply_expert(): pl.pallas_call(expert_kernel, out_shape=(out, out), in_specs=[vmem] * 3 +...]
where the time goes in v4:
time: 55.8 us; the launch traced here: 55.5 us
  waiting for transfers between devices  15.9 us (28%)
  blocking collectives  14.3 us (26%)
  Pallas kernels  13.8 us (25%)
  starting transfers between devices  8.18 us (15%)
  other arithmetic  2.3 us (4%)
  local copies, waits for them, and re-layouts  0.83 us (1%)
    all_to_all x1, blocking collectives, per_device(): lax.all_to_all(outgoing, 'ep', split_axis=0, concat_axis=0, tiled=True)  14.3 us
    all_to_all x1, waiting for transfers between devices, per_device(): lax.all_to_all(pieces, ('y', 'ep'), split_axis=0, concat_axis=0, tiled=True)  10.1 us
    pallas_call x1, Pallas kernels, attend(): pl.pallas_call(attention_kernel, out_shape=(out, out), in_specs=[hbm] * 1...  9.47 us
    all_to_all x1, starting transfers between devices, per_device(): lax.all_to_all(pieces, ('y', 'ep'), split_axis=0, concat_axis=0, tiled=True)  4.5 us
    pallas_call x1, Pallas kernels, apply_expert(): pl.pallas_call(expert_kernel, out_shape=(out, out), in_specs=[vmem] * 3 +...  4.32 us
    ppermute x3, waiting for transfers between devices, swap_cores(): return lax.ppermute(source, 'core', [(0, 1), (1, 0)])  3.96 us
    ppermute x1, starting transfers between devices, per_device(): other = lax.ppermute(pair, 'y', [(0, 1), (1, 0)])  2.92 us
    ppermute x1, waiting for transfers between devices, per_device(): other = lax.ppermute(pair, 'y', [(0, 1), (1, 0)])  1.82 us
  transfers between devices with their start and end apart: 5, of which 5 were waited for; matrix products, arithmetic and copies ran while one was open for 0% of the time, Pallas kernels for 0%

profile of v4, /device:TPU:0, one launch (start us, length us, event | category | flops | bytes accessed | tf_op | source)
XLA Modules:
  0.0 55.5 jit_solution(16675239309320064133)
XLA Ops:
  0.0 0.0 copy-start.1
  0.0 0.0 copy-start
  0.0 9.5 %attention.1 = (bf16[2,16,512]{2,1,0:T(8,128)(2,1)}, bf16[2,16,512]{2,1,0:T(8,128)(2,1)}) custom-call(s32[16]{0:T(128)} %lengths_hbm.1, f32[2]{0:T(128)} %lambda_hbm.1, bf16[16,2048]{1,0:T(8,128)(2,1)} %tokens_hbm.1, f32[1,2048]{1,0:T(1,128)} %bitcast.44, f32[1,128]{1,0:T(1,128)} %bitcast.45, bf16[4096,128]{1,0:T(8,128)(2,1)} %bitcast.36, ...), custom_call_target="tpu_custom_call" | custom-call | flops 4000000000 | bytes 16777216 | tf_op jit(solution)/shard_map/attention/pallas_call | solution.py:232
  9.5 0.6 %collective-permute-start = (bf16[2,16,512]{2,1,0:T(8,128)(2,1)}, bf16[2,16,512]{2,1,0:T(8,128)(2,1)S(1)}, u32[]{:S(2)}, u32[]{:S(2)}) collective-permute-start(bf16[2,16,512]{2,1,0:T(8,128)(2,1)} %get-tuple-element.10), channel_id=1, source_target_pairs={{0,1},{1,0},{2,3},{3,2},{4,5},{5,4},{6,7},{7,6},{8,9},{9,8},{10,11... | collective-permute-start | bytes 98312 | tf_op jit(solution)/shard_map/ppermute | solution.py:406
  10.0 0.0 copy-done.1
  10.1 1.0 %collective-permute-done = bf16[2,16,512]{2,1,0:T(8,128)(2,1)S(1)} collective-permute-done((bf16[2,16,512]{2,1,0:T(8,128)(2,1)}, bf16[2,16,512]{2,1,0:T(8,128)(2,1)S(1)}, u32[]{:S(2)}, u32[]{:S(2)}) %collective-permute-start) | collective-permute-done | bytes 32800 | tf_op jit(solution)/shard_map/ppermute | solution.py:406
  11.1 0.8 %add_convert_fusion.1 = bf16[2,16,512]{2,1,0:T(8,128)(2,1)S(1)} fusion(bf16[2,16,512]{2,1,0:T(8,128)(2,1)S(1)} %collective-permute-done, bf16[2,16,512]{2,1,0:T(8,128)(2,1)} %get-tuple-element.9), kind=kLoop, calls=%fused_computation.4 | loop fusion | flops 65536 | bytes 98304 | tf_op jit(solution)/shard_map/convert_element_type | solution.py:410
  11.9 2.9 %collective-permute-start.1 = (bf16[2,16,512]{2,1,0:T(8,128)(2,1)S(1)}, bf16[2,16,512]{2,1,0:T(8,128)(2,1)S(1)}, u32[]{:S(2)}, u32[]{:S(2)}) collective-permute-start(bf16[2,16,512]{2,1,0:T(8,128)(2,1)S(1)} %add_convert_fusion.1), channel_id=1, source_target_pairs={{0,2},{2,0},{1,3},{3,1},{4,6},{6,4},{5,7},{7,5},{8,10},{10,8},{9,1... | collective-permute-start | bytes 98312 | tf_op jit(solution)/shard_map/ppermute | solution.py:428
  14.8 0.1 constant_dynamic-slice_fusion
  14.9 1.8 %collective-permute-done.1 = bf16[2,16,512]{2,1,0:T(8,128)(2,1)S(1)} collective-permute-done((bf16[2,16,512]{2,1,0:T(8,128)(2,1)S(1)}, bf16[2,16,512]{2,1,0:T(8,128)(2,1)S(1)}, u32[]{:S(2)}, u32[]{:S(2)}) %collective-permute-start.1) | collective-permute-done | bytes 32800 | tf_op jit(solution)/shard_map/ppermute | solution.py:428
  16.8 14.3 %all_to_all.10 = bf16[8,16,1024]{2,1,0:T(8,128)(2,1)S(1)} all-to-all(bf16[8,16,1024]{2,1,0:T(8,128)(2,1)S(1)} %broadcast_in_dim.26), channel_id=1, replica_groups=mesh['ep'=8,'y'=2,'core'=2] {'ep'}, dimensions={0} | all-to-all | bytes 524288 | tf_op jit(solution)/shard_map/all_to_all | solution.py:451
  31.1 0.0 collective-permute-start.2
  31.1 1.5 %collective-permute-done.2.other_ref = bf16[128,1024]{1,0:T(8,128)(2,1)S(1)} collective-permute-done((bf16[128,1024]{1,0:T(8,128)(2,1)S(1)}, bf16[128,1024]{1,0:T(8,128)(2,1)S(1)}, u32[]{:S(2)}, u32[]{:S(2)}) %collective-permute-start.2) | collective-permute-done | bytes 262176 | tf_op jit(solution)/shard_map/ppermute | solution.py:406
  32.6 0.0 copy-start.2
  32.6 0.7 %copy-done.2 = bf16[128,1024]{1,0:T(8,128)(2,1)} copy-done((bf16[128,1024]{1,0:T(8,128)(2,1)}, bf16[128,1024]{1,0:T(8,128)(2,1)S(1)}, u32[]{:S(2)}) %copy-start.2) | copy-done | bytes 262168
  33.3 0.0 copy-done
  33.3 0.0 copy-start.3
  33.3 0.0 copy-start.4
  33.3 4.3 %expert.1 = (bf16[2,128,512]{2,1,0:T(8,128)(2,1)S(1)}, bf16[2,128,512]{2,1,0:T(8,128)(2,1)S(1)}) custom-call(bf16[128,1024]{1,0:T(8,128)(2,1)S(1)} %bitcast.29, bf16[128,1024]{1,0:T(8,128)(2,1)} %copy-done.2, f32[1,2048]{1,0:T(1,128)S(1)} %bitcast.30, bf16[2048,512]{1,0:T(8,128)(2,1)} %bitcast.33, bf16[2048,512]{1,0:T(8,128)(2,1)} %bitcast.34, ...), custom_call_target="tpu_custom_call" | custom-call | flops 805306368 | bytes 6291456 | tf_op jit(solution)/shard_map/expert/pallas_call | solution.py:348
  37.7 0.2 collective-permute-start.3
  37.9 1.4 %collective-permute-done.3 = bf16[2,128,512]{2,1,0:T(8,128)(2,1)S(1)} collective-permute-done((bf16[2,128,512]{2,1,0:T(8,128)(2,1)S(1)}, bf16[2,128,512]{2,1,0:T(8,128)(2,1)S(1)}, u32[]{:S(2)}, u32[]{:S(2)}) %collective-permute-start.3) | collective-permute-done | bytes 262176 | tf_op jit(solution)/shard_map/ppermute | solution.py:406
  39.3 0.8 %add_convert_fusion = bf16[2,128,512]{2,1,0:T(8,128)(2,1)} fusion(bf16[2,128,512]{2,1,0:T(8,128)(2,1)S(1)} %collective-permute-done.3, bf16[2,128,512]{2,1,0:T(8,128)(2,1)S(1)} %get-tuple-element.11), kind=kLoop, calls=%fused_computation | loop fusion | flops 524288 | bytes 786432 | tf_op jit(solution)/shard_map/convert_element_type | solution.py:410
  40.0 4.5 %all-to-all-start.1 = ((bf16[16,16,512]{2,1,0:T(8,128)(2,1)}), bf16[16,16,512]{2,1,0:T(8,128)(2,1)S(1)}, u32[]{:S(2)}, u32[]{:S(2)}) async-start(bf16[16,16,512]{2,1,0:T(8,128)(2,1)} %bitcast.17), calls=%async_computation.1 | async-start | bytes 524288 | tf_op jit(solution)/shard_map/all_to_all | solution.py:457
  44.5 0.0 copy-done.3
  44.5 0.0 copy-done.4
  44.6 10.1 %all-to-all-done.1 = bf16[16,16,512]{2,1,0:T(8,128)(2,1)S(1)} async-done(((bf16[16,16,512]{2,1,0:T(8,128)(2,1)}), bf16[16,16,512]{2,1,0:T(8,128)(2,1)S(1)}, u32[]{:S(2)}, u32[]{:S(2)}) %all-to-all-start.1) | async-done | bytes 262176 | tf_op jit(solution)/shard_map/all_to_all | solution.py:457
  54.7 0.1 multiply_reduce_fusion
  54.8 0.6 %fusion.1 = bf16[16,512]{1,0:T(8,128)(2,1)} fusion(f32[16,512]{1,0:T(8,128)S(1)} %multiply_reduce_fusion, bf16[16,2,512]{2,0,1:T(8,128)(2,1)S(1)} %fusion, s32[]{:T(128)S(6)} %select_n.13), kind=kLoop, calls=%fused_computation.7 | loop fusion | flops 24576 | bytes 65540 | tf_op jit(solution)/shard_map/convert_element_type | solution.py:470
  (6 shorter events, 0.1 us)
Async XLA Ops:
  0.0 10.0 %copy-start.1 = (bf16[16,2048]{1,0:T(8,128)(2,1)S(1)}, bf16[16,2048]{1,0:T(8,128)(2,1)}, u32[]{:S(2)}) copy-start(bf16[16,2048]{1,0:T(8,128)(2,1)} %tokens_hbm.1) | copy-start | bytes 196612
  0.0 33.3 %copy-start = (f32[2048]{0:T(1024)S(1)}, f32[2048]{0:T(1024)}, u32[]{:S(2)}) copy-start(f32[2048]{0:T(1024)} %param.28) | copy-start | bytes 24580
  9.5 1.6 %collective-permute-start = (bf16[2,16,512]{2,1,0:T(8,128)(2,1)}, bf16[2,16,512]{2,1,0:T(8,128)(2,1)S(1)}, u32[]{:S(2)}, u32[]{:S(2)}) collective-permute-start(bf16[2,16,512]{2,1,0:T(8,128)(2,1)} %get-tuple-element.10), channel_id=1, source_target_pairs={{0,1},{1,0},{2,3},{3,2},{4,5},{5,4},{6,7},{7,6},{8,9},{9,8},{10,11... | collective-permute-start | bytes 98312 | tf_op jit(solution)/shard_map/ppermute | solution.py:406
  11.9 4.8 %collective-permute-start.1 = (bf16[2,16,512]{2,1,0:T(8,128)(2,1)S(1)}, bf16[2,16,512]{2,1,0:T(8,128)(2,1)S(1)}, u32[]{:S(2)}, u32[]{:S(2)}) collective-permute-start(bf16[2,16,512]{2,1,0:T(8,128)(2,1)S(1)} %add_convert_fusion.1), channel_id=1, source_target_pairs={{0,2},{2,0},{1,3},{3,1},{4,6},{6,4},{5,7},{7,5},{8,10},{10,8},{9,1... | collective-permute-start | bytes 98312 | tf_op jit(solution)/shard_map/ppermute | solution.py:428
  31.1 1.5 %collective-permute-start.2 = (bf16[128,1024]{1,0:T(8,128)(2,1)S(1)}, bf16[128,1024]{1,0:T(8,128)(2,1)S(1)}, u32[]{:S(2)}, u32[]{:S(2)}) collective-permute-start(bf16[128,1024]{1,0:T(8,128)(2,1)S(1)} %bitcast.28), channel_id=1, source_target_pairs={{0,1},{1,0},{2,3},{3,2},{4,5},{5,4},{6,7},{7,6},{8,9},{9,8},{10,11... | collective-permute-start | bytes 786440 | tf_op jit(solution)/shard_map/ppermute | solution.py:406
  32.6 0.7 %copy-start.2 = (bf16[128,1024]{1,0:T(8,128)(2,1)}, bf16[128,1024]{1,0:T(8,128)(2,1)S(1)}, u32[]{:S(2)}) copy-start(bf16[128,1024]{1,0:T(8,128)(2,1)S(1)} %collective-permute-done.2.other_ref) | copy-start | bytes 786436
  33.3 11.2 %copy-start.3 = (f32[16,4]{0,1:T(4,128)S(1)}, f32[16,4]{0,1:T(4,128)}, u32[]{:S(2)}) copy-start(f32[16,4]{0,1:T(4,128)} %param.33) | copy-start | bytes 772
  33.3 11.2 %copy-start.4 = (s32[16,4]{0,1:T(4,128)S(1)}, s32[16,4]{0,1:T(4,128)}, u32[]{:S(2)}) copy-start(s32[16,4]{0,1:T(4,128)} %param.32) | copy-start | bytes 772
  37.7 1.6 %collective-permute-start.3 = (bf16[2,128,512]{2,1,0:T(8,128)(2,1)S(1)}, bf16[2,128,512]{2,1,0:T(8,128)(2,1)S(1)}, u32[]{:S(2)}, u32[]{:S(2)}) collective-permute-start(bf16[2,128,512]{2,1,0:T(8,128)(2,1)S(1)} %get-tuple-element.12), channel_id=1, source_target_pairs={{0,1},{1,0},{2,3},{3,2},{4,5},{5,4},{6,7},{7,6},{8,9},{9,8},{10,11... | collective-permute-start | bytes 786440 | tf_op jit(solution)/shard_map/ppermute | solution.py:406
  40.0 14.7 %all-to-all-start.1 = ((bf16[16,16,512]{2,1,0:T(8,128)(2,1)}), bf16[16,16,512]{2,1,0:T(8,128)(2,1)S(1)}, u32[]{:S(2)}, u32[]{:S(2)}) async-start(bf16[16,16,512]{2,1,0:T(8,128)(2,1)} %bitcast.17), calls=%async_computation.1 | async-start | bytes 524288 | tf_op jit(solution)/shard_map/all_to_all | solution.py:457
